TPU v7x, 32 devices: a whole 2x2x4 slice. The times are simulated.
32 devices in a mesh: grp: 2 (over y), sp: 4 (over z), tp: 4 (over x, core).
Axes of the slice: x: 2, y: 2, z: 4, core: 2. Of those that a mesh axis runs over, the one named last changes fastest.
Arguments:
- tokens: bfloat16 [256, 8, 2048], P(('sp', 'tp'), 'grp'), parts along dimension 1, may hold values from -6 to 6
- norm_gain: float32 [2048], replicated, may hold values from 0.1 to 1.9
- w_query: bfloat16 [2048, 2048], P('sp', 'tp'), may hold values from -0.125 to 0.125
- w_value: bfloat16 [2048, 2048], P('sp', 'tp'), may hold values from -0.125 to 0.125
- w_fwd_gate: bfloat16 [2048, 2048], P('sp', 'tp'), may hold values from -0.125 to 0.125
- w_bwd_gate: bfloat16 [2048, 2048], P('sp', 'tp'), may hold values from -0.125 to 0.125
- w_out_gate: bfloat16 [2048, 2048], P('sp', 'tp'), may hold values from -0.125 to 0.125
- floor_gap: float32 [2, 2048], P(None, 'tp'), may hold values from 0.00078125 to 0.1
- decay_shift: float32 [256, 8, 2048], P('sp', 'grp', 'tp'), parts along dimension 1, may hold values from -1.1 to 0
- head_gain: float32 [128], replicated, may hold values from 0.1 to 1.9
- w_out: bfloat16 [2048, 2048], P('tp', 'sp'), may hold values from -0.125 to 0.125
Outputs:
- layer_out: bfloat16 [256, 8, 2048], P(('sp', 'tp'), 'grp'), parts along dimension 1
There are 2 independent parts, one for each index of `grp`. A program takes and returns all parts, laid end to end along the dimension named above; an argument that names none is the same for every part. Nothing has to cross between parts.
All inputs are finite; a program needn't handle non-finite values.
Results may differ from a plain program's by a relative error of at most 0.013.
Values may be sent and summed in bfloat16 or wider, within the bound.
A program may use at most 128 MiB of HBM per device.

v0:
```python
import functools

import jax
import jax.numpy as jnp
from jax import lax
from jax.experimental import pallas as pl
from jax.experimental.pallas import tpu as pltpu
from jax.sharding import PartitionSpec as P

KEY = 128
VAL = 128
BLOCK = 64


norm_eps = 1e-06
highest = lax.Precision.HIGHEST


def carried_in(x, axis, join, neutral, backward):
    count = lax.axis_size(axis)
    place = lax.axis_index(axis)
    ahead = count - 1 - place if backward else place
    gathered = jax.tree.map(
        lambda a, kind: lax.all_gather(a.astype(kind), axis), x, (jnp.bfloat16, jnp.bfloat16)
    )
    state = jax.tree.map(lambda a, e: jnp.zeros_like(a) + jnp.asarray(e, a.dtype), x, neutral)

    def one(turn, state):
        source = count - 1 - turn if backward else turn
        return join(
            state,
            jax.tree.map(
                lambda a, own: lax.dynamic_index_in_dim(a, source, 0, False).astype(own.dtype),
                gathered,
                x,
            ),
        )

    return lax.fori_loop(0, ahead, one, state)


def split_blocks(array):
    return array.reshape(array.shape[0] // BLOCK, BLOCK, *array.shape[1:])


def prepare_chain(queries, key_cols, values, log_decay):
    query_blocks = split_blocks(queries)
    key_blocks = split_blocks(key_cols)
    value_blocks = split_blocks(values)
    running = jnp.cumsum(split_blocks(log_decay), axis=1)
    block_end = running[:, -1]
    block_state = jnp.einsum(
        "nsbhk,nsbhe->nbhke",
        key_blocks * jnp.exp(block_end[:, None] - running),
        value_blocks,
        precision=highest,
    )
    carry_state = jnp.zeros_like(block_state[0])
    log_total = jnp.zeros_like(block_end[0])
    offsets = [log_total]
    carry_state = jnp.exp(block_end[0])[..., None] * carry_state + block_state[0]
    log_total = block_end[0]
    return (
        query_blocks,
        key_blocks,
        value_blocks,
        running,
        block_state,
        jnp.stack(offsets),
        log_total,
        carry_state,
    )


def local_pass(chain, carry_state):
    query_blocks, key_blocks, value_blocks, running, block_state = (
        chain[0],
        chain[1],
        chain[2],
        chain[3],
        chain[4],
    )
    block_len = running.shape[1]
    earlier_mask = jnp.arange(block_len)[:, None] >= jnp.arange(block_len)[None, :]
    here = running[0]
    anchor = here[:1]
    query_scaled = query_blocks[0] * jnp.exp(here - anchor)
    key_scaled = key_blocks[0] * jnp.exp(anchor - here)
    scores = jnp.einsum("tbhk,sbhk->bhts", query_scaled, key_scaled, precision=highest)
    scores = jnp.where(earlier_mask, scores, 0.0)
    within = jnp.einsum("bhts,sbhe->tbhe", scores, value_blocks[0], precision=highest)
    carried = jnp.einsum(
        "tbhk,bhke->tbhe", query_blocks[0] * jnp.exp(here), carry_state, precision=highest
    )
    outputs = within + carried
    return outputs


def combine(earlier, later):
    return (earlier[0] + later[0], jnp.exp(later[0])[..., None] * earlier[1] + later[1])


def group_sums(flat_mixed, weight_lines, group_count):
    group_width = flat_mixed.shape[1] // group_count
    accumulated_total = jnp.zeros((flat_mixed.shape[0], weight_lines.shape[1]), jnp.float32)
    for tp_group in range(group_count):
        first_column = tp_group * group_width
        partial_value = jnp.dot(
            flat_mixed[:, first_column : first_column + group_width],
            weight_lines[first_column : first_column + group_width],
            preferred_element_type=jnp.float32,
        ).astype(jnp.bfloat16)
        accumulated_total = accumulated_total + lax.optimization_barrier(partial_value).astype(
            jnp.float32
        )
    return accumulated_total


def shards(
    tokens,
    norm_gain,
    w_query,
    w_value,
    w_fwd_gate,
    w_bwd_gate,
    w_out_gate,
    floor_gap,
    decay_shift,
    head_gain,
    w_out,
):
    token_f32 = tokens.astype(jnp.float32)
    scale_rows = lax.rsqrt(jnp.mean(token_f32 * token_f32, axis=-1, keepdims=True) + norm_eps)
    normed = (token_f32 * scale_rows * norm_gain).astype(jnp.bfloat16)
    weights = (
        lax.all_gather(w_query, "sp", axis=0, tiled=True),
        lax.all_gather(w_value, "sp", axis=0, tiled=True),
        lax.all_gather(w_fwd_gate, "sp", axis=0, tiled=True),
        lax.all_gather(w_bwd_gate, "sp", axis=0, tiled=True),
        lax.all_gather(w_out_gate, "sp", axis=0, tiled=True),
    )
    piece_rows = lax.all_gather(normed, "tp", axis=0, tiled=True)
    flat_rows = piece_rows.reshape(-1, piece_rows.shape[2])
    columns = [
        jnp.dot(flat_rows, matrix, preferred_element_type=jnp.float32).astype(jnp.bfloat16)
        for matrix in weights
    ]
    projected = lax.optimization_barrier(
        jnp.concatenate(columns, axis=1).reshape(piece_rows.shape[0], piece_rows.shape[1], -1)
    )
    key_width = w_query.shape[1]
    value_width = w_value.shape[1]
    heads_here = key_width // KEY
    extent_rows = projected.shape[0]
    seq_count = projected.shape[1]
    bounds_list = [
        0,
        key_width,
        key_width + value_width,
        2 * key_width + value_width,
        3 * key_width + value_width,
        3 * key_width + 2 * value_width,
    ]

    def section_part(position, feature_lanes):
        picked = projected[:, :, bounds_list[position] : bounds_list[position + 1]].astype(
            jnp.float32
        )
        return picked.reshape(extent_rows, seq_count, heads_here, feature_lanes)

    queries = jax.nn.silu(section_part(0, KEY))
    values = section_part(1, VAL)
    shift = decay_shift.reshape(extent_rows, seq_count, heads_here, KEY)
    key_fwd = floor_gap[0].reshape(heads_here, KEY) * jax.nn.sigmoid(-section_part(2, KEY))
    key_bwd = floor_gap[1].reshape(heads_here, KEY) * jax.nn.sigmoid(-section_part(3, KEY))
    decay_fwd = jnp.log1p(-key_fwd) + shift
    decay_bwd = jnp.log1p(-key_bwd) + shift
    fwd_chain = prepare_chain(queries, key_fwd, values, decay_fwd)
    bwd_chain = prepare_chain(queries[::-1], key_bwd[::-1], values[::-1], decay_bwd[::-1])
    identity_pair = (jnp.zeros_like(fwd_chain[6]), jnp.zeros_like(fwd_chain[7]))
    fwd_in = carried_in((fwd_chain[6], fwd_chain[7]), "sp", combine, identity_pair, False)[1]
    bwd_in = carried_in((bwd_chain[6], bwd_chain[7]), "sp", combine, identity_pair, True)[1]
    out_fwd = local_pass(fwd_chain, fwd_in)
    out_bwd = local_pass(bwd_chain, bwd_in)
    combined = out_fwd + out_bwd[::-1]
    head_normed = (
        combined
        * lax.rsqrt(jnp.mean(combined * combined, axis=-1, keepdims=True) + norm_eps)
        * head_gain
    )
    gate_value = jax.nn.silu(projected[:, :, bounds_list[4] : bounds_list[5]].astype(jnp.float32))
    mixed = (head_normed.reshape(extent_rows, seq_count, value_width) * gate_value).astype(
        jnp.bfloat16
    )
    token_rows = lax.all_to_all(mixed, "tp", split_axis=0, concat_axis=2, tiled=True)
    flat_mixed = token_rows.reshape(-1, token_rows.shape[2])
    group_count = lax.axis_size("tp")
    w_columns = lax.all_gather(w_out, "sp", axis=1, tiled=True)
    w_full = lax.all_gather(w_columns, "tp", axis=0, tiled=True)
    accumulated_total = group_sums(flat_mixed, w_full, group_count)
    result = accumulated_total.reshape(token_rows.shape[0], token_rows.shape[1], -1)
    return result.astype(jnp.bfloat16)


MESH = pl.DeviceIdType.MESH
CORES = 2


def greet(peers):
    barrier = pltpu.get_barrier_semaphore()
    for peer in peers:
        pl.semaphore_signal(barrier, inc=1, device_id=peer, device_id_type=MESH)
    pl.semaphore_wait(barrier, len(peers))


def gather_phase(
    sizes,
    xn_ref,
    shift_ref,
    wq_ref,
    wv_ref,
    wf_ref,
    wb_ref,
    wg_ref,
    proj_ref,
    acts,
    weights,
    shifts,
    own_sem,
    az_sem,
    ax_sem,
    ac_sem,
    wz_sem,
    wy_sem,
    sz_sem,
):
    n_grp, n_sp, n_tp = sizes
    n_x = n_tp // CORES
    g = lax.axis_index("grp")
    s = lax.axis_index("sp")
    t = lax.axis_index("tp")
    x = t // CORES
    c = t % CORES
    seqs, span = xn_ref.shape[0], xn_ref.shape[1]
    depth = wq_ref.shape[0]
    part = depth // n_grp
    positions = shift_ref.shape[1]
    sources = (wq_ref, wv_ref, wf_ref, wb_ref, wg_ref)

    z_at = [s] + [lax.rem(s + k, n_sp) for k in range(1, n_sp)]
    z_from = [s] + [lax.rem(s + n_sp - k, n_sp) for k in range(1, n_sp)]
    x_at = [t] + [lax.rem(x + j, n_x) * CORES + c for j in range(1, n_x)]
    x_from = [t] + [lax.rem(x + n_x - j, n_x) * CORES + c for j in range(1, n_x)]
    twin = x * CORES + (1 - c)
    y_at = [g] + [lax.rem(g + m, n_grp) for m in range(1, n_grp)]
    y_from = [g] + [lax.rem(g + n_grp - m, n_grp) for m in range(1, n_grp)]

    def block(where_s, where_t):
        return acts.at[:, pl.ds(pl.multiple_of((where_s * n_tp + where_t) * span, span), span), :]

    def remote(src, dst, sems, index, peer):
        return pltpu.make_async_remote_copy(
            src_ref=src,
            dst_ref=dst,
            send_sem=sems.at[(0, *index)],
            recv_sem=sems.at[(1, *index)],
            device_id=peer,
            device_id_type=MESH,
        )

    def rows(where_s, where_g):
        return pl.ds(pl.multiple_of(where_s * depth + where_g * part, part), part)

    def lanes(where):
        return pl.ds(pl.multiple_of(where * KEY, KEY), KEY)

    mine = [
        pltpu.make_async_copy(
            w.at[:, lanes(s)],
            weights.at[pl.ds(pl.multiple_of(s * depth, depth), depth), pl.ds(p * KEY, KEY)],
            own_sem.at[p],
        )
        for p, w in enumerate(sources)
    ]
    mine.append(
        pltpu.make_async_copy(
            shift_ref.at[:, :, lanes(s)],
            shifts.at[:, pl.ds(pl.multiple_of(s * positions, positions), positions), :],
            own_sem.at[len(sources)],
        )
    )

    sent = []

    def go(copy):
        copy.start()
        sent.append(copy)
        return copy

    def slot(up, d):
        return 1 + d if up else n_sp + d

    def chain(up, d):
        step = -1 if up else 1
        there = s - step
        sends = jnp.logical_and(
            jnp.logical_and(there >= 0, there < n_sp),
            jnp.logical_and(s + step * d >= 0, s + step * d < n_sp),
        )
        gets = jnp.logical_and(s + step * (d + 1) >= 0, s + step * (d + 1) < n_sp)
        return there, s + step * d, sends, s + step * (d + 1), gets

    def act_move(up, d, from_own):
        there, origin, _, _, _ = chain(up, d)
        src = block(origin, t)
        return remote(src, block(origin, t), az_sem, (slot(up, d) - 1,), (g, there, t))

    def act_spread(kind, j, index, where_s, where_t, from_own):
        src = block(where_s, where_t)
        if kind == "x":
            return remote(src, block(where_s, where_t), ax_sem, (j - 1, index), (g, s, x_at[j]))
        return remote(src, block(where_s, where_t), ac_sem, (j, index), (g, s, twin))

    for up in (True, False):
        _, _, sends, _, _ = chain(up, 0)

        @pl.when(sends)
        def _():
            act_move(up, 0, True).start()

    for j in range(1, n_x):
        act_spread("x", j, 0, s, t, True).start()
    act_spread("c", 0, 0, s, t, True).start()
    for copy in mine:
        copy.start()

    w_z = {}

    def send_weights(p):
        for k in range(1, n_sp):
            w_z[k, p] = go(
                remote(
                    sources[p].at[pl.ds(pl.multiple_of(g * part, part), part), lanes(z_at[k])],
                    weights.at[rows(s, g), pl.ds(p * KEY, KEY)],
                    wz_sem,
                    (k - 1, p),
                    (g, z_at[k], t),
                )
            )

    w_y = {}

    def swap(p):
        for k in range(1, n_sp):
            w_z[k, p].wait_recv()
            here = weights.at[rows(z_from[k], g), pl.ds(p * KEY, KEY)]
            for m in range(1, n_grp):
                w_y[m, k, p] = go(remote(here, here, wy_sem, (m - 1, k - 1, p), (y_at[m], s, t)))

    queue = list(range(len(sources)))
    for d in range(n_sp - 1):
        if queue and d >= 1:
            send_weights(queue.pop(0))
        for up in (True, False):
            _, _, _, origin, gets = chain(up, d)

            @pl.when(gets)
            def _():
                act_move(up, d, False).wait_recv()
                if d + 1 < n_sp - 1:
                    _, _, sends, _, _ = chain(up, d + 1)

                    @pl.when(sends)
                    def _():
                        act_move(up, d + 1, False).start()

                for j in range(1, n_x):
                    act_spread("x", j, slot(up, d), origin, t, False).start()
                act_spread("c", 0, slot(up, d), origin, t, False).start()

        if d == n_sp - 2:
            for p in queue:
                send_weights(p)
            queue = []
        if d >= 2:
            swap(d - 2)

    s_z = {}
    for k in range(1, n_sp):
        s_z[k] = go(
            remote(
                shift_ref.at[:, :, lanes(z_at[k])],
                shifts.at[:, pl.ds(pl.multiple_of(s * positions, positions), positions), :],
                sz_sem,
                (k - 1,),
                (g, z_at[k], t),
            )
        )

    def each_block(visit, ds=None):
        if ds is None:
            visit(0, s)
        for d in range(n_sp - 1) if ds is None else ds:
            for up in (True, False):
                _, _, _, origin, gets = chain(up, d)

                @pl.when(gets)
                def _():
                    visit(slot(up, d), origin)

    def relay(index, origin):
        for j in range(1, n_x):
            act_spread("x", j, index, origin, t, False).wait_recv()
            act_spread("c", j, index, origin, x_from[j], False).start()

    relay(0, s)
    left = list(range(max(n_sp - 3, 0), len(sources)))
    for d in range(n_sp - 1):
        each_block(relay, [d])
        if left:
            swap(left.pop(0))
    for p in left:
        swap(p)
    for copy in mine:
        copy.wait()

    def joined(index, origin):
        for j in range(n_x):
            act_spread("c", j, index, origin, t, False).wait_recv()

    each_block(joined)
    for first in range(0, len(sources), 2):
        last = min(first + 2, len(sources))
        for (m, k, p), copy in w_y.items():
            if first <= p < last:
                copy.wait_recv()
        at = slice(first * KEY, last * KEY)

        def project(q, carry):
            proj_ref[q, :, at] = jnp.dot(
                acts[q], weights[:, at], preferred_element_type=jnp.float32
            ).astype(jnp.bfloat16)
            return carry

        lax.fori_loop(0, seqs, project, 0)
    for copy in s_z.values():
        copy.wait_recv()
    for d in range(n_sp - 1):
        for up in (True, False):
            _, _, sends, _, _ = chain(up, d)

            @pl.when(sends)
            def _():
                act_move(up, d, d == 0).wait_send()

    def gone(index, origin):
        for j in range(1, n_x):
            act_spread("x", j, index, origin, t, False).wait_send()
        for j in range(n_x):
            act_spread("c", j, index, origin, x_from[j], False).wait_send()

    each_block(gone)
    for copy in sent:
        copy.wait_send()


def recur_one(proj_ref, shift_ref, gap_ref, gain_ref, out_ref, i, own):
    f32 = jnp.float32
    bf16 = jnp.bfloat16
    length = proj_ref.shape[1]

    def cols(p):
        return proj_ref[i, :, p * KEY : (p + 1) * KEY]

    queries = cols(0).astype(f32)
    queries = queries * jax.nn.sigmoid(queries)
    values = cols(1)
    shift = shift_ref[i].astype(f32)
    row = lax.broadcasted_iota(jnp.int32, (length, length), 0)
    col = lax.broadcasted_iota(jnp.int32, (length, length), 1)
    near = row // BLOCK == col // BLOCK
    row = lax.broadcasted_iota(jnp.int32, (BLOCK, BLOCK), 0)
    col_b = lax.broadcasted_iota(jnp.int32, (BLOCK, BLOCK), 1)
    seen = [row >= col_b, row <= col_b]
    row_l = lax.broadcasted_iota(jnp.int32, (length, length), 0)
    order = [row_l >= col, row_l <= col]
    blocks = length // BLOCK
    keys, here = [], []
    for d in range(2):
        key = gap_ref[d : d + 1, own] * jax.nn.sigmoid(-cols(2 + d).astype(f32))
        decay = jnp.log1p(-key) + shift
        high = decay.astype(bf16)
        rest = decay - high.astype(f32)
        middle = rest.astype(bf16)
        low = (rest - middle.astype(f32)).astype(bf16)
        tri = jnp.where(jnp.logical_and(near, order[d]), 1.0, 0.0).astype(bf16)
        sums = jnp.dot(
            tri, jnp.concatenate([high, middle, low], axis=1), preferred_element_type=f32
        )
        here.append(sums[:, :KEY] + (sums[:, KEY : 2 * KEY] + sums[:, 2 * KEY :]))
        keys.append(key)
    state = [None, None]
    outs = [[None, None] for _ in range(blocks)]
    for step in range(blocks):
        for d in range(2):
            n = step if d == 0 else blocks - 1 - step
            at = slice(n * BLOCK, (n + 1) * BLOCK)
            q, k, v, h = queries[at], keys[d][at], values[at], here[d][at]
            edge = h[BLOCK - 1 : BLOCK] if d == 0 else h[0:1]
            anchor = h[BLOCK // 2 : BLOCK // 2 + 1]
            scores = lax.dot_general(
                (q * jnp.exp(h - anchor)).astype(bf16),
                (k * jnp.exp(anchor - h)).astype(bf16),
                (((1,), (1,)), ((), ())),
                preferred_element_type=f32,
            )
            scores = jnp.where(seen[d], scores, 0.0).astype(bf16)
            out = jnp.dot(scores, v, preferred_element_type=f32)
            if state[d] is not None:
                out = out + lax.dot_general(
                    (q * jnp.exp(h)).astype(bf16),
                    state[d].astype(bf16),
                    (((1,), (1,)), ((), ())),
                    preferred_element_type=f32,
                )
            outs[n][d] = out
            if step < blocks - 1:
                fresh = lax.dot_general(
                    v,
                    (k * jnp.exp(edge - h)).astype(bf16),
                    (((0,), (0,)), ((), ())),
                    preferred_element_type=f32,
                )
                state[d] = fresh if state[d] is None else state[d] * jnp.exp(edge) + fresh
    for n in range(blocks):
        out_ref[n * BLOCK : (n + 1) * BLOCK] = outs[n][0] + outs[n][1]
    combined = out_ref[...]
    normed = combined * lax.rsqrt(jnp.mean(combined * combined, axis=-1, keepdims=True) + norm_eps)
    gate = cols(4).astype(f32)
    return (normed * gain_ref[...] * (gate * jax.nn.sigmoid(gate))).astype(bf16)


def mix_phase(
    sizes,
    proj_ref,
    shift_ref,
    gap_ref,
    gain_ref,
    w_ref,
    out_ref,
    summed,
    heads,
    matrix,
    partial,
    landed,
    own_sem,
    w_sem,
    z_sem,
    c_sem,
    p_sem,
):
    n_grp, n_sp, n_tp = sizes
    n_x = n_tp // CORES
    g = lax.axis_index("grp")
    s = lax.axis_index("sp")
    t = lax.axis_index("tp")
    x = t // CORES
    c = t % CORES
    twin = x * CORES + (1 - c)
    seqs = proj_ref.shape[0]
    span = out_ref.shape[1]
    depth, width = w_ref.shape[0], w_ref.shape[1] // CORES
    half = seqs // 2
    z_at = [lax.rem(s + k, n_sp) for k in range(n_sp)]
    t_at = [lax.rem(t + j, n_tp) for j in range(n_tp)]
    others = [(k, j) for k in range(n_sp) for j in range(n_tp) if k or j]

    def lanes(where, size):
        return pl.ds(pl.multiple_of(where * size, size), size)

    def remote(src, dst, sems, index, peer):
        return pltpu.make_async_remote_copy(
            src_ref=src,
            dst_ref=dst,
            send_sem=sems.at[(0, *index)],
            recv_sem=sems.at[(1, *index)],
            device_id=peer,
            device_id_type=MESH,
        )

    w_rows = pl.ds(pl.multiple_of(c * depth, depth), depth)
    w_own = pltpu.make_async_copy(w_ref.at[:, lanes(c, width)], matrix.at[w_rows, :], own_sem)
    w_twin = remote(w_ref.at[:, lanes(1 - c, width)], matrix.at[w_rows, :], w_sem, (), (g, s, twin))
    w_own.start()
    w_twin.start()

    def head(q, where):
        return heads.at[q, :, lanes(c * n_sp + where, VAL)]

    def slot(up, d):
        return 1 + d if up else n_sp + d

    def inside(place):
        return jnp.logical_and(place >= 0, place < n_sp)

    def z_move(q, up, d):
        step = 1 if up else -1
        here = head(q, s - step * d)
        return remote(here, here, z_sem, (q, slot(up, d) - 1), (g, s + step, t))

    def z_sends(up, d):
        step = 1 if up else -1
        return jnp.logical_and(inside(s + step), inside(s - step * d))

    def z_gets(up, d):
        step = 1 if up else -1
        return inside(s - step * (d + 1))

    def c_move(q, index, origin):
        here = head(q, origin)
        return remote(here, here, c_sem, (q, index), (g, s, twin))

    def each(d, visit):
        for up in (True, False):

            @pl.when(z_gets(up, d))
            def _():
                visit(up, s - (d + 1) if up else s + (d + 1))

    def arrived(q, d):
        def visit(up, origin):
            z_move(q, up, d).wait_recv()
            if d + 1 < n_sp - 1:

                @pl.when(z_sends(up, d + 1))
                def _():
                    z_move(q, up, d + 1).start()

            c_move(q, slot(up, d), origin).start()

        each(d, visit)

    def advance(q, carry):
        heads[q, :, lanes(c * n_sp + s, VAL)] = recur_one(
            proj_ref, shift_ref, gap_ref, gain_ref, summed, q, lanes(s, KEY)
        )
        for up in (True, False):

            @pl.when(z_sends(up, 0))
            def _():
                z_move(q, up, 0).start()

        c_move(q, 0, s).start()
        for d in range(n_sp - 1):

            @pl.when(q >= d + 1)
            def _():
                arrived(q - (d + 1), d)

        return carry

    lax.fori_loop(0, seqs, advance, 0)

    def piece(where_s, where_t):
        return pl.ds(pl.multiple_of((where_s * n_tp + where_t) * span, span), span)

    def p_move(h, k, j):
        both = pl.ds(h * half, half)
        return remote(
            partial.at[both, piece(z_at[k], t_at[j]), :],
            landed.at[x, both, :, lanes(s * CORES + c, width)],
            p_sem,
            (h, k, j),
            (g, z_at[k], t_at[j]),
        )

    def finish(h):
        def one(q, carry):
            c_move(q, 0, s).wait_recv()
            for d in range(n_sp - 1):
                each(d, lambda up, origin: c_move(q, slot(up, d), origin).wait_recv())
            partial[q] = jnp.dot(
                heads[q], matrix[...], preferred_element_type=jnp.float32
            ).astype(jnp.bfloat16)
            return carry

        lax.fori_loop(h * half, (h + 1) * half, one, 0)
        for k, j in others:
            p_move(h, k, j).start()
        both = pl.ds(h * half, half)
        landed[x, both, :, lanes(s * CORES + c, width)] = partial[both, piece(s, t), :]

    w_own.wait()
    w_twin.wait_recv()
    pending = [
        (i - 1 - d, d)
        for i in range(seqs, seqs + n_sp - 1)
        for d in range(n_sp - 1)
        if 0 <= i - 1 - d < seqs
    ]
    early = [item for item in pending if item[0] < half]
    late = [item for item in pending if item[0] >= half]
    cut = pending.index(early[-1]) + 1 if early else 0
    for q, d in pending[:cut]:
        arrived(q, d)
    finish(0)
    for q, d in pending[cut:]:
        arrived(q, d)
    finish(1)
    for h in range(2):
        for k, j in others:
            p_move(h, k, j).wait_recv()
    total = landed[0].astype(jnp.float32)
    for j in range(1, n_x):
        total = total + landed[j].astype(jnp.float32)
    out_ref[...] = total.astype(jnp.bfloat16)

    w_twin.wait_send()

    def drain(q, carry):
        c_move(q, 0, s).wait_send()
        for d in range(n_sp - 1):
            each(d, lambda up, origin: c_move(q, slot(up, d), origin).wait_send())
            for up in (True, False):

                @pl.when(z_sends(up, d))
                def _():
                    z_move(q, up, d).wait_send()

        return carry

    lax.fori_loop(0, seqs, drain, 0)
    for h in range(2):
        for k, j in others:
            p_move(h, k, j).wait_send()


def layer_kernel(
    sizes,
    xn_ref,
    norm_ref,
    shift_ref,
    wq_ref,
    wv_ref,
    wf_ref,
    wb_ref,
    wg_ref,
    gap_ref,
    gain_ref,
    w_ref,
    out_ref,
    proj,
    acts,
    weights,
    shifts,
    summed,
    heads,
    matrix,
    partial,
    landed,
    own_sem,
    az_sem,
    ax_sem,
    ac_sem,
    wz_sem,
    wy_sem,
    sz_sem,
    mix_own_sem,
    mix_w_sem,
    mix_z_sem,
    mix_c_sem,
    mix_p_sem,
):
    n_grp, n_sp, n_tp = sizes
    g = lax.axis_index("grp")
    s = lax.axis_index("sp")
    t = lax.axis_index("tp")
    peers = [
        (g, lax.rem(s + k, n_sp), lax.rem(t + j, n_tp))
        for k in range(n_sp)
        for j in range(n_tp)
        if k or j
    ]
    peers += [(lax.rem(g + m, n_grp), s, t) for m in range(1, n_grp)]
    span = xn_ref.shape[1]
    rows = xn_ref[...].astype(jnp.float32)
    scale = lax.rsqrt(jnp.mean(rows * rows, axis=-1, keepdims=True) + norm_eps)
    acts[:, pl.ds(pl.multiple_of((s * n_tp + t) * span, span), span), :] = (
        rows * scale * norm_ref[...]
    ).astype(jnp.bfloat16)
    greet(peers)
    gather_phase(
        sizes,
        xn_ref,
        shift_ref,
        wq_ref,
        wv_ref,
        wf_ref,
        wb_ref,
        wg_ref,
        proj,
        acts,
        weights,
        shifts,
        own_sem,
        az_sem,
        ax_sem,
        ac_sem,
        wz_sem,
        wy_sem,
        sz_sem,
    )
    mix_phase(
        sizes,
        proj,
        shifts,
        gap_ref,
        gain_ref,
        w_ref,
        out_ref,
        summed,
        heads,
        matrix,
        partial,
        landed,
        mix_own_sem,
        mix_w_sem,
        mix_z_sem,
        mix_c_sem,
        mix_p_sem,
    )


def layer(sizes, xn, norm_gain, shift, sources, gap, gain, w_out):
    n_grp, n_sp, n_tp = sizes
    n_x = n_tp // CORES
    seqs, span, model = xn.shape
    length = n_sp * n_tp * span
    count = len(sources)
    depth, width = w_out.shape
    part = width // CORES
    dma = pltpu.SemaphoreType.DMA
    hbm = pl.BlockSpec(memory_space=pltpu.HBM)
    vmem = pl.BlockSpec(memory_space=pltpu.VMEM)
    return pl.pallas_call(
        functools.partial(layer_kernel, sizes),
        out_shape=jax.ShapeDtypeStruct((seqs, span, n_sp * width), jnp.bfloat16),
        in_specs=[vmem, vmem] + [hbm] * (1 + count) + [vmem, vmem, hbm],
        out_specs=vmem,
        scratch_shapes=[
            pltpu.VMEM((seqs, length, count * KEY), jnp.bfloat16),
            pltpu.VMEM((seqs, length, model), jnp.bfloat16),
            pltpu.VMEM((model, count * KEY), jnp.bfloat16),
            pltpu.VMEM((seqs, length, KEY), shift.dtype),
            pltpu.VMEM((length, VAL), jnp.float32),
            pltpu.VMEM((seqs, length, CORES * depth), jnp.bfloat16),
            pltpu.VMEM((CORES * depth, part), jnp.bfloat16),
            pltpu.VMEM((seqs, length, part), jnp.bfloat16),
            pltpu.VMEM((n_x, seqs, span, n_sp * width), jnp.bfloat16),
            dma((count + 1,)),
            dma((2, 2 * n_sp - 2)),
            dma((2, max(n_x - 1, 1), 2 * n_sp - 1)),
            dma((2, n_x, 2 * n_sp - 1)),
            dma((2, n_sp - 1, count)),
            dma((2, max(n_grp - 1, 1), n_sp - 1, count)),
            dma((2, n_sp - 1)),
            dma,
            dma((2,)),
            dma((2, seqs, 2 * n_sp - 2)),
            dma((2, seqs, 2 * n_sp - 1)),
            dma((2, 2, n_sp, n_tp)),
        ],
        compiler_params=pltpu.CompilerParams(
            collective_id=0, has_side_effects=True, vmem_limit_bytes=56 * 1024 * 1024
        ),
    )(xn, norm_gain, shift, *sources, gap, gain, w_out)


def head_shards(
    sizes,
    tokens,
    norm_gain,
    w_query,
    w_value,
    w_fwd_gate,
    w_bwd_gate,
    w_out_gate,
    floor_gap,
    decay_shift,
    head_gain,
    w_out,
):
    return layer(
        sizes,
        tokens.transpose(1, 0, 2),
        norm_gain.reshape(1, 1, -1),
        decay_shift.astype(jnp.bfloat16).transpose(1, 0, 2),
        (w_query, w_value, w_fwd_gate, w_bwd_gate, w_out_gate),
        floor_gap,
        head_gain.reshape(1, VAL),
        w_out,
    ).transpose(1, 0, 2)


def by_heads(mesh):
    n_sp, n_tp = mesh.shape["sp"], mesh.shape["tp"]

    def run(*arrays):
        tokens, w_query = arrays[0], arrays[2]
        heads_here = w_query.shape[1] // KEY // n_tp
        span = tokens.shape[0] // (n_sp * n_tp)
        sizes = (mesh.shape["grp"], n_sp, n_tp)
        fits = heads_here == n_sp and n_sp > 1 and n_tp % CORES == 0 and span % 16 == 0
        fits = fits and tokens.shape[1] // sizes[0] % 2 == 0
        fits = fits and tokens.shape[0] % BLOCK == 0 and tokens.shape[0] <= 512
        body = functools.partial(head_shards, sizes) if fits else shards
        return mapped(body, mesh)(*arrays)

    return run


def mapped(body, mesh):
    return jax.shard_map(
        body,
        mesh=mesh,
        in_specs=(
            P(("sp", "tp"), "grp", None),
            P(),
            P("sp", "tp"),
            P("sp", "tp"),
            P("sp", "tp"),
            P("sp", "tp"),
            P("sp", "tp"),
            P(None, "tp"),
            P("sp", "grp", "tp"),
            P(),
            P("tp", "sp"),
        ),
        out_specs=P(("sp", "tp"), "grp", None),
        check_vma=False,
    )


def solution(mesh):
    return by_heads(mesh)
```

profile of v0, /device:TPU:0, one launch (start us, length us, event | category | flops | bytes accessed | tf_op | source)
XLA Modules:
  0.0 95.3 jit_solution(10452576126806556290)
XLA Ops:
  0.0 0.0 copy-start
  0.0 1.9 %copy.20 = bf16[16,4,2048]{2,0,1:T(8,128)(2,1)} copy(bf16[16,4,2048]{2,1,0:T(4,128)(2,1)} %param.11) | data formatting | bytes 524288 | tf_op args[0]
  1.9 0.0 copy-done
  1.9 0.8 copy.19
  2.7 90.7 %shard_map.109 = bf16[4,16,2048]{2,1,0:T(8,128)(2,1)} custom-call(bf16[4,16,2048]{2,1,0:T(8,128)(2,1)} %bitcast.11, f32[1,1,2048]{2,1,0:T(1,128)} %bitcast.12, bf16[4,64,512]{2,1,0:T(8,128)(2,1)} %bitcast.9, bf16[512,512]{1,0:T(8,128)(2,1)} %wq_ref.1, bf16[512,512]{1,0:T(8,128)(2,1)} %wv_ref.1, bf16[512,512]{1,0:T(8,128)(2,1)} %wf_ref.1, ...), custom_call_target="tpu_custom_call" | custom-call | tf_op jit(solution)/shard_map/pallas_call | solution.py:845
  93.5 1.9 %copy.14 = bf16[16,4,2048]{2,1,0:T(4,128)(2,1)} copy(bf16[16,4,2048]{2,0,1:T(8,128)(2,1)} %bitcast.10) | data formatting | bytes 524288 | tf_op jit(solution)/shard_map/transpose | solution.py:902
Async XLA Ops:
  0.0 1.9 %copy-start = (f32[64,4,512]{2,1,0:T(4,128)S(1)}, f32[64,4,512]{2,1,0:T(4,128)}, u32[]{:S(2)}) copy-start(f32[64,4,512]{2,1,0:T(4,128)} %param.19) | copy-start | bytes 1572868
where the time goes:
time: 95.7 us; the launch traced here: 95.3 us
  Pallas kernels  90.7 us (95%)
  local copies, waits for them, and re-layouts  4.56 us (5%)
    pallas_call x1, Pallas kernels, layer(): pl.pallas_call(functools.partial(layer_kernel, sizes), out_shape=jax.Shap...  90.7 us
    unnamed x4, local copies, waits for them, and re-layouts  2.7 us

commit v1 on v0

v1 whole, which is shorter than its diff:
```python
import functools

import jax
import jax.numpy as jnp
from jax import lax
from jax.experimental import pallas as pl
from jax.experimental.pallas import tpu as pltpu
from jax.sharding import PartitionSpec as P

KEY = 128
VAL = 128
BLOCK = 64


norm_eps = 1e-06
highest = lax.Precision.HIGHEST


def carried_in(x, axis, join, neutral, backward):
    count = lax.axis_size(axis)
    place = lax.axis_index(axis)
    ahead = count - 1 - place if backward else place
    gathered = jax.tree.map(
        lambda a, kind: lax.all_gather(a.astype(kind), axis), x, (jnp.bfloat16, jnp.bfloat16)
    )
    state = jax.tree.map(lambda a, e: jnp.zeros_like(a) + jnp.asarray(e, a.dtype), x, neutral)

    def one(turn, state):
        source = count - 1 - turn if backward else turn
        return join(
            state,
            jax.tree.map(
                lambda a, own: lax.dynamic_index_in_dim(a, source, 0, False).astype(own.dtype),
                gathered,
                x,
            ),
        )

    return lax.fori_loop(0, ahead, one, state)


def split_blocks(array):
    return array.reshape(array.shape[0] // BLOCK, BLOCK, *array.shape[1:])


def prepare_chain(queries, key_cols, values, log_decay):
    query_blocks = split_blocks(queries)
    key_blocks = split_blocks(key_cols)
    value_blocks = split_blocks(values)
    running = jnp.cumsum(split_blocks(log_decay), axis=1)
    block_end = running[:, -1]
    block_state = jnp.einsum(
        "nsbhk,nsbhe->nbhke",
        key_blocks * jnp.exp(block_end[:, None] - running),
        value_blocks,
        precision=highest,
    )
    carry_state = jnp.zeros_like(block_state[0])
    log_total = jnp.zeros_like(block_end[0])
    offsets = [log_total]
    carry_state = jnp.exp(block_end[0])[..., None] * carry_state + block_state[0]
    log_total = block_end[0]
    return (
        query_blocks,
        key_blocks,
        value_blocks,
        running,
        block_state,
        jnp.stack(offsets),
        log_total,
        carry_state,
    )


def local_pass(chain, carry_state):
    query_blocks, key_blocks, value_blocks, running, block_state = (
        chain[0],
        chain[1],
        chain[2],
        chain[3],
        chain[4],
    )
    block_len = running.shape[1]
    earlier_mask = jnp.arange(block_len)[:, None] >= jnp.arange(block_len)[None, :]
    here = running[0]
    anchor = here[:1]
    query_scaled = query_blocks[0] * jnp.exp(here - anchor)
    key_scaled = key_blocks[0] * jnp.exp(anchor - here)
    scores = jnp.einsum("tbhk,sbhk->bhts", query_scaled, key_scaled, precision=highest)
    scores = jnp.where(earlier_mask, scores, 0.0)
    within = jnp.einsum("bhts,sbhe->tbhe", scores, value_blocks[0], precision=highest)
    carried = jnp.einsum(
        "tbhk,bhke->tbhe", query_blocks[0] * jnp.exp(here), carry_state, precision=highest
    )
    outputs = within + carried
    return outputs


def combine(earlier, later):
    return (earlier[0] + later[0], jnp.exp(later[0])[..., None] * earlier[1] + later[1])


def group_sums(flat_mixed, weight_lines, group_count):
    group_width = flat_mixed.shape[1] // group_count
    accumulated_total = jnp.zeros((flat_mixed.shape[0], weight_lines.shape[1]), jnp.float32)
    for tp_group in range(group_count):
        first_column = tp_group * group_width
        partial_value = jnp.dot(
            flat_mixed[:, first_column : first_column + group_width],
            weight_lines[first_column : first_column + group_width],
            preferred_element_type=jnp.float32,
        ).astype(jnp.bfloat16)
        accumulated_total = accumulated_total + lax.optimization_barrier(partial_value).astype(
            jnp.float32
        )
    return accumulated_total


def shards(
    tokens,
    norm_gain,
    w_query,
    w_value,
    w_fwd_gate,
    w_bwd_gate,
    w_out_gate,
    floor_gap,
    decay_shift,
    head_gain,
    w_out,
):
    token_f32 = tokens.astype(jnp.float32)
    scale_rows = lax.rsqrt(jnp.mean(token_f32 * token_f32, axis=-1, keepdims=True) + norm_eps)
    normed = (token_f32 * scale_rows * norm_gain).astype(jnp.bfloat16)
    weights = (
        lax.all_gather(w_query, "sp", axis=0, tiled=True),
        lax.all_gather(w_value, "sp", axis=0, tiled=True),
        lax.all_gather(w_fwd_gate, "sp", axis=0, tiled=True),
        lax.all_gather(w_bwd_gate, "sp", axis=0, tiled=True),
        lax.all_gather(w_out_gate, "sp", axis=0, tiled=True),
    )
    piece_rows = lax.all_gather(normed, "tp", axis=0, tiled=True)
    flat_rows = piece_rows.reshape(-1, piece_rows.shape[2])
    columns = [
        jnp.dot(flat_rows, matrix, preferred_element_type=jnp.float32).astype(jnp.bfloat16)
        for matrix in weights
    ]
    projected = lax.optimization_barrier(
        jnp.concatenate(columns, axis=1).reshape(piece_rows.shape[0], piece_rows.shape[1], -1)
    )
    key_width = w_query.shape[1]
    value_width = w_value.shape[1]
    heads_here = key_width // KEY
    extent_rows = projected.shape[0]
    seq_count = projected.shape[1]
    bounds_list = [
        0,
        key_width,
        key_width + value_width,
        2 * key_width + value_width,
        3 * key_width + value_width,
        3 * key_width + 2 * value_width,
    ]

    def section_part(position, feature_lanes):
        picked = projected[:, :, bounds_list[position] : bounds_list[position + 1]].astype(
            jnp.float32
        )
        return picked.reshape(extent_rows, seq_count, heads_here, feature_lanes)

    queries = jax.nn.silu(section_part(0, KEY))
    values = section_part(1, VAL)
    shift = decay_shift.reshape(extent_rows, seq_count, heads_here, KEY)
    key_fwd = floor_gap[0].reshape(heads_here, KEY) * jax.nn.sigmoid(-section_part(2, KEY))
    key_bwd = floor_gap[1].reshape(heads_here, KEY) * jax.nn.sigmoid(-section_part(3, KEY))
    decay_fwd = jnp.log1p(-key_fwd) + shift
    decay_bwd = jnp.log1p(-key_bwd) + shift
    fwd_chain = prepare_chain(queries, key_fwd, values, decay_fwd)
    bwd_chain = prepare_chain(queries[::-1], key_bwd[::-1], values[::-1], decay_bwd[::-1])
    identity_pair = (jnp.zeros_like(fwd_chain[6]), jnp.zeros_like(fwd_chain[7]))
    fwd_in = carried_in((fwd_chain[6], fwd_chain[7]), "sp", combine, identity_pair, False)[1]
    bwd_in = carried_in((bwd_chain[6], bwd_chain[7]), "sp", combine, identity_pair, True)[1]
    out_fwd = local_pass(fwd_chain, fwd_in)
    out_bwd = local_pass(bwd_chain, bwd_in)
    combined = out_fwd + out_bwd[::-1]
    head_normed = (
        combined
        * lax.rsqrt(jnp.mean(combined * combined, axis=-1, keepdims=True) + norm_eps)
        * head_gain
    )
    gate_value = jax.nn.silu(projected[:, :, bounds_list[4] : bounds_list[5]].astype(jnp.float32))
    mixed = (head_normed.reshape(extent_rows, seq_count, value_width) * gate_value).astype(
        jnp.bfloat16
    )
    token_rows = lax.all_to_all(mixed, "tp", split_axis=0, concat_axis=2, tiled=True)
    flat_mixed = token_rows.reshape(-1, token_rows.shape[2])
    group_count = lax.axis_size("tp")
    w_columns = lax.all_gather(w_out, "sp", axis=1, tiled=True)
    w_full = lax.all_gather(w_columns, "tp", axis=0, tiled=True)
    accumulated_total = group_sums(flat_mixed, w_full, group_count)
    result = accumulated_total.reshape(token_rows.shape[0], token_rows.shape[1], -1)
    return result.astype(jnp.bfloat16)


MESH = pl.DeviceIdType.MESH
CORES = 2
PIECES = 2


def recur_one(proj_ref, shift_ref, gap_ref, gain_ref, out_ref, i, own):
    f32 = jnp.float32
    bf16 = jnp.bfloat16
    length = proj_ref.shape[1]

    def cols(p):
        return proj_ref[i, :, p * KEY : (p + 1) * KEY]

    queries = cols(0).astype(f32)
    queries = queries * jax.nn.sigmoid(queries)
    values = cols(1)
    shift = shift_ref[i].astype(f32)
    row = lax.broadcasted_iota(jnp.int32, (length, length), 0)
    col = lax.broadcasted_iota(jnp.int32, (length, length), 1)
    near = row // BLOCK == col // BLOCK
    row = lax.broadcasted_iota(jnp.int32, (BLOCK, BLOCK), 0)
    col_b = lax.broadcasted_iota(jnp.int32, (BLOCK, BLOCK), 1)
    seen = [row >= col_b, row <= col_b]
    row_l = lax.broadcasted_iota(jnp.int32, (length, length), 0)
    order = [row_l >= col, row_l <= col]
    blocks = length // BLOCK
    keys, here = [], []
    for d in range(2):
        key = gap_ref[d : d + 1, own] * jax.nn.sigmoid(-cols(2 + d).astype(f32))
        decay = jnp.log1p(-key) + shift
        high = decay.astype(bf16)
        rest = decay - high.astype(f32)
        middle = rest.astype(bf16)
        low = (rest - middle.astype(f32)).astype(bf16)
        tri = jnp.where(jnp.logical_and(near, order[d]), 1.0, 0.0).astype(bf16)
        sums = jnp.dot(
            tri, jnp.concatenate([high, middle, low], axis=1), preferred_element_type=f32
        )
        here.append(sums[:, :KEY] + (sums[:, KEY : 2 * KEY] + sums[:, 2 * KEY :]))
        keys.append(key)
    state = [None, None]
    outs = [[None, None] for _ in range(blocks)]
    for step in range(blocks):
        for d in range(2):
            n = step if d == 0 else blocks - 1 - step
            at = slice(n * BLOCK, (n + 1) * BLOCK)
            q, k, v, h = queries[at], keys[d][at], values[at], here[d][at]
            edge = h[BLOCK - 1 : BLOCK] if d == 0 else h[0:1]
            anchor = h[BLOCK // 2 : BLOCK // 2 + 1]
            scores = lax.dot_general(
                (q * jnp.exp(h - anchor)).astype(bf16),
                (k * jnp.exp(anchor - h)).astype(bf16),
                (((1,), (1,)), ((), ())),
                preferred_element_type=f32,
            )
            scores = jnp.where(seen[d], scores, 0.0).astype(bf16)
            out = jnp.dot(scores, v, preferred_element_type=f32)
            if state[d] is not None:
                out = out + lax.dot_general(
                    (q * jnp.exp(h)).astype(bf16),
                    state[d].astype(bf16),
                    (((1,), (1,)), ((), ())),
                    preferred_element_type=f32,
                )
            outs[n][d] = out
            if step < blocks - 1:
                fresh = lax.dot_general(
                    v,
                    (k * jnp.exp(edge - h)).astype(bf16),
                    (((0,), (0,)), ((), ())),
                    preferred_element_type=f32,
                )
                state[d] = fresh if state[d] is None else state[d] * jnp.exp(edge) + fresh
    for n in range(blocks):
        combined = outs[n][0] + outs[n][1]
        scale = lax.rsqrt(jnp.mean(combined * combined, axis=-1, keepdims=True) + norm_eps)
        out_ref[i, n * BLOCK : (n + 1) * BLOCK] = combined * scale * gain_ref[...]


def layer_kernel(
    sizes,
    token_ref,
    norm_ref,
    shift_ref,
    wq_ref,
    wv_ref,
    wf_ref,
    wb_ref,
    wg_ref,
    gap_ref,
    gain_ref,
    w_ref,
    out_ref,
    rows_in,
    wide,
    raw_shift,
    own_shift,
    shifts,
    acts,
    weights,
    proj,
    summed,
    mixed,
    heads,
    matrix,
    partial,
    landed,
    load_sem,
    own_sem,
    az_sem,
    ax_sem,
    ac_sem,
    wz_sem,
    wy_sem,
    sz_sem,
    oz_sem,
    oy_sem,
    oc_sem,
    m_sem,
    p_sem,
):
    bf16 = jnp.bfloat16
    f32 = jnp.float32
    n_grp, n_sp, n_tp = sizes
    n_x = n_tp // CORES
    g = lax.axis_index("grp")
    s = lax.axis_index("sp")
    t = lax.axis_index("tp")
    x = t // CORES
    c = t % CORES
    twin = x * CORES + (1 - c)
    across = (1 - x) * CORES + c
    seqs = acts.shape[0]
    span = token_ref.shape[0]
    positions = n_tp * span
    depth = wq_ref.shape[0]
    half = depth // n_grp
    width = w_ref.shape[1]
    lot = seqs // PIECES
    sources = (wq_ref, wv_ref, wf_ref, wb_ref, wg_ref)
    count = len(sources)
    last = n_sp - 1
    z_at = [lax.rem(s + k, n_sp) for k in range(n_sp)]
    z_from = [lax.rem(s + n_sp - k, n_sp) for k in range(n_sp)]
    core_at = [c, 1 - c]

    def lanes(where, size=KEY):
        return pl.ds(pl.multiple_of(where * size, size), size)

    def remote(src, dst, sems, index, peer):
        return pltpu.make_async_remote_copy(
            src_ref=src,
            dst_ref=dst,
            send_sem=sems.at[(0, *index)],
            recv_sem=sems.at[(1, *index)],
            device_id=peer,
            device_id_type=MESH,
        )

    def inside(place):
        return jnp.logical_and(place >= 0, place < n_sp)

    def step_of(up):
        return 1 if up else -1

    def slot(up, d):
        return 1 + d if up else n_sp + d

    def sends(up, d):
        return jnp.logical_and(inside(s + step_of(up)), inside(s - step_of(up) * d))

    def gets(up, d):
        return inside(s - step_of(up) * (d + 1))

    def each(d, visit):
        for up in (True, False):

            @pl.when(gets(up, d))
            def _():
                visit(up, d, s - step_of(up) * (d + 1))

    sent = []

    def go(copy):
        copy.start()
        sent.append(copy)
        return copy

    load_rows = pltpu.make_async_copy(token_ref, rows_in, load_sem.at[0])
    load_shift = pltpu.make_async_copy(shift_ref, raw_shift, load_sem.at[1])
    load_rows.start()
    load_shift.start()
    peers = [(g, z_at[k], x * CORES + core_at[o]) for k in range(n_sp) for o in range(CORES)]
    peers = peers[1:] + [(g, s, across), (1 - g, s, t)]
    barrier = pltpu.get_barrier_semaphore()
    for peer in peers:
        pl.semaphore_signal(barrier, inc=1, device_id=peer, device_id_type=MESH)
    mine = [
        pltpu.make_async_copy(
            w.at[:, lanes(s)],
            weights.at[pl.ds(pl.multiple_of(s * depth, depth), depth), pl.ds(p * KEY, KEY)],
            own_sem.at[p],
        )
        for p, w in enumerate(sources)
    ]
    w_rows = pl.ds(pl.multiple_of(c * depth, depth), depth)
    w_own = pltpu.make_async_copy(w_ref, matrix.at[w_rows, lanes(s, width)], own_sem.at[count])
    for copy in mine:
        copy.start()
    w_own.start()

    here_rows = pl.ds(pl.multiple_of((s * n_tp + t) * span, span), span)
    load_rows.wait()
    rows = rows_in[...].astype(f32)
    scale = lax.rsqrt(jnp.mean(rows * rows, axis=-1, keepdims=True) + norm_eps)
    wide[...] = rows * scale * norm_ref[...]
    for q in range(seqs):
        acts[q, here_rows, :] = wide[:, q, :].astype(bf16)
    pl.semaphore_wait(barrier, len(peers))

    def block(where_s, where_t, piece):
        at = pl.ds(pl.multiple_of((where_s * n_tp + where_t) * span, span), span)
        return acts.at[pl.ds(piece * lot, lot), at, :]

    def act_z(up, d, piece):
        here = block(s - step_of(up) * d, t, piece)
        return remote(here, here, az_sem, (slot(up, d) - 1, piece), (g, s + step_of(up), t))

    def act_x(index, origin, piece):
        here = block(origin, t, piece)
        return remote(here, here, ax_sem, (index, piece), (g, s, across))

    def act_c(far, index, origin, piece):
        here = block(origin, across if far else t, piece)
        return remote(here, here, ac_sem, (far, index, piece), (g, s, twin))

    for piece in range(PIECES):
        for up in (True, False):

            @pl.when(sends(up, 0))
            def _():
                act_z(up, 0, piece).start()

        act_x(0, s, piece).start()
    for piece in range(PIECES):
        act_c(0, 0, s, piece).start()

    load_shift.wait()
    for q in range(seqs):
        values = raw_shift[:, q, :].astype(bf16)
        for k in range(n_sp):
            own_shift[k, q] = values[:, k * KEY : (k + 1) * KEY]
    place = pl.ds(pl.multiple_of(s * positions, positions), positions)
    shifts[:, place, :] = own_shift[s]

    part = pl.ds(pl.multiple_of(g * half, half), half)

    def w_rows_of(where_s, where_g):
        return pl.ds(pl.multiple_of(where_s * depth + where_g * half, half), half)

    def w_z(k, p):
        return remote(
            sources[p].at[part, lanes(z_at[k])],
            weights.at[w_rows_of(s, g), pl.ds(p * KEY, KEY)],
            wz_sem,
            (k - 1, p),
            (g, z_at[k], t),
        )

    def w_y(k, p):
        here = weights.at[w_rows_of(z_from[k], g), pl.ds(p * KEY, KEY)]
        return remote(here, here, wy_sem, (k - 1, p), (1 - g, s, t))

    def s_z(k):
        return remote(own_shift.at[z_at[k]], shifts.at[:, place, :], sz_sem, (k - 1,), (g, z_at[k], t))

    def o_block(where_s, where_g, where_c):
        at = pl.ds(pl.multiple_of(where_c * depth + where_g * half, half), half)
        return matrix.at[at, lanes(where_s, width)]

    def o_z(up, d):
        origin = s - step_of(up) * d
        here = o_block(origin, g, c)
        src = w_ref.at[part, :] if d == 0 else here
        return remote(src, here, oz_sem, (slot(up, d) - 1,), (g, s + step_of(up), t))

    def o_y(index, origin):
        here = o_block(origin, g, c)
        return remote(here, here, oy_sem, (index - 1,), (1 - g, s, t))

    def o_c(far, index, origin):
        here = o_block(origin, 1 - g if far else g, c)
        return remote(here, here, oc_sem, (far, index), (g, s, twin))

    def o_own():
        at = matrix.at[w_rows, lanes(s, width)]
        return remote(w_ref, at, oc_sem, (0, 0), (g, s, twin))

    def issue(up):
        def ahead(visit):
            for k in range(1, n_sp):
                go_up = s + k < n_sp

                @pl.when(go_up if up else jnp.logical_not(go_up))
                def _():
                    visit(k)

        for p in range(count - 1):
            ahead(lambda k: w_z(k, p).start())
        ahead(lambda k: s_z(k).start())

        @pl.when(sends(up, 0))
        def _():
            o_z(up, 0).start()

        ahead(lambda k: w_z(k, count - 1).start())

    for up in (True, False):

        @pl.when(s == (0 if up else last))
        def _():
            issue(up)

    for d in range(last):
        for piece in range(PIECES):

            def arrived(up, d, origin):
                act_z(up, d, piece).wait_recv()
                if d + 1 < last:

                    @pl.when(sends(up, d + 1))
                    def _():
                        act_z(up, d + 1, piece).start()

                act_x(slot(up, d), origin, piece).start()
                act_c(0, slot(up, d), origin, piece).start()

            each(d, arrived)
        if d + 1 < last:
            for up in (True, False):

                @pl.when(s == (d + 1 if up else last - 1 - d))
                def _():
                    issue(up)

    o_own().start()

    def relay(index, origin):
        for piece in range(PIECES):
            act_x(index, origin, piece).wait_recv()
            act_c(1, index, origin, piece).start()

    def swap(p):
        for k in range(1, n_sp):
            w_z(k, p).wait_recv()
            go(w_y(k, p))

    relay(0, s)
    for d in range(last):
        each(d, lambda up, d, origin: relay(slot(up, d), origin))
        if d < 2:
            swap(d)

    def joined(index, origin):
        for piece in range(PIECES):
            for far in range(2):
                act_c(far, index, origin, piece).wait_recv()

    joined(0, s)
    for d in range(last):
        each(d, lambda up, d, origin: joined(slot(up, d), origin))
    for copy in mine:
        copy.wait()

    def project(first, end):
        for p in range(first, end):
            for k in range(1, n_sp):
                w_y(k, p).wait_recv()
        at = slice(first * KEY, end * KEY)

        def one(q, carry):
            proj[q, :, at] = jnp.dot(
                acts[q], weights[:, at], preferred_element_type=f32
            ).astype(bf16)
            return carry

        lax.fori_loop(0, seqs, one, 0)

    def o_arrived(up, d, origin):
        o_z(up, d).wait_recv()
        if d + 1 < last:

            @pl.when(sends(up, d + 1))
            def _():
                o_z(up, d + 1).start()

        o_y(slot(up, d), origin).start()
        o_c(0, slot(up, d), origin).start()

    def o_swapped(up, d, origin):
        o_y(slot(up, d), origin).wait_recv()
        o_c(1, slot(up, d), origin).start()

    def recur(q, carry):
        recur_one(proj, shifts, gap_ref, gain_ref, summed, q, lanes(s))
        return carry

    swap(2)
    project(0, 2)
    swap(3)
    project(2, 4)
    for k in range(1, n_sp):
        s_z(k).wait_recv()
    lax.fori_loop(0, seqs // 2, recur, 0)
    each(0, o_arrived)
    swap(4)
    lax.fori_loop(seqs // 2, seqs, recur, 0)
    each(1, o_arrived)
    each(0, o_swapped)
    project(4, 5)

    targets = [(k, o) for k in range(n_sp) for o in range(CORES) if k or o]

    def m_move(q, k, o):
        return remote(
            mixed.at[q, z_at[k], :, core_at[o]],
            heads.at[:, q, :, lanes(c * n_sp + s, VAL)],
            m_sem,
            (q, k, o),
            (g, z_at[k], x * CORES + core_at[o]),
        )

    def mix(q, carry):
        gate = proj[q, :, 4 * KEY : 5 * KEY].astype(f32)
        value = (summed[q] * (gate * jax.nn.sigmoid(gate))).astype(bf16)
        mixed[q] = value.reshape(n_sp, n_x, CORES, span, VAL)
        heads[:, q, :, lanes(c * n_sp + s, VAL)] = mixed[q, s, :, c]
        for k, o in targets:
            m_move(q, k, o).start()
        return carry

    lax.fori_loop(0, seqs, mix, 0)
    for d in range(2, last):
        each(d, o_arrived)
    for d in range(1, last):
        each(d, o_swapped)
    w_own.wait()
    o_own().wait_recv()

    def o_joined(up, d, origin):
        for far in range(2):
            o_c(far, slot(up, d), origin).wait_recv()

    for d in range(last):
        each(d, o_joined)

    strips = matrix.shape[1] // width

    def p_move(h, n):
        both = pl.ds(h * lot, lot)
        at = pl.ds(n * width, width)
        return remote(
            partial.at[1 - x, both, :, at],
            landed.at[both, :, at],
            p_sem,
            (h, n),
            (g, s, across),
        )

    for h in range(PIECES):
        both = slice(h * lot, (h + 1) * lot)
        for q in range(h * lot, (h + 1) * lot):
            for k, o in targets:
                m_move(q, k, o).wait_recv()
        lines = heads[:, both].reshape(n_x * lot * span, -1)
        for n in range(strips):
            at = slice(n * width, (n + 1) * width)
            partial[:, both, :, at] = (
                jnp.dot(lines, matrix[:, at], preferred_element_type=f32)
                .astype(bf16)
                .reshape(n_x, lot, span, width)
            )
            go(p_move(h, n))
    for h in range(PIECES):
        for n in range(strips):
            p_move(h, n).wait_recv()
        for q in range(h * lot, (h + 1) * lot):
            wide[:, q, :] = partial[x, q].astype(f32) + landed[q].astype(f32)
    out_ref[...] = wide[...].astype(bf16)

    for copy in sent:
        copy.wait_send()
    for k in range(1, n_sp):
        s_z(k).wait_send()
        for p in range(count):
            w_z(k, p).wait_send()
    o_own().wait_send()
    for piece in range(PIECES):
        act_x(0, s, piece).wait_send()
        for far in range(2):
            act_c(far, 0, s, piece).wait_send()
    for d in range(last):
        for up in (True, False):

            @pl.when(sends(up, d))
            def _():
                o_z(up, d).wait_send()
                for piece in range(PIECES):
                    act_z(up, d, piece).wait_send()

        def gone(up, d, origin):
            o_y(slot(up, d), origin).wait_send()
            for far in range(2):
                o_c(far, slot(up, d), origin).wait_send()
            for piece in range(PIECES):
                act_x(slot(up, d), origin, piece).wait_send()
                for far in range(2):
                    act_c(far, slot(up, d), origin, piece).wait_send()

        each(d, gone)

    def drain(q, carry):
        for k, o in targets:
            m_move(q, k, o).wait_send()
        return carry

    lax.fori_loop(0, seqs, drain, 0)


def layer(sizes, tokens, norm_gain, shift, sources, gap, gain, w_out):
    n_grp, n_sp, n_tp = sizes
    n_x = n_tp // CORES
    span, seqs, model = tokens.shape
    length = n_sp * n_tp * span
    count = len(sources)
    depth, width = w_out.shape
    slots = 2 * n_sp - 1
    strips = n_sp
    dma = pltpu.SemaphoreType.DMA
    hbm = pl.BlockSpec(memory_space=pltpu.HBM)
    vmem = pl.BlockSpec(memory_space=pltpu.VMEM)
    bf16 = jnp.bfloat16
    return pl.pallas_call(
        functools.partial(layer_kernel, sizes),
        out_shape=jax.ShapeDtypeStruct((span, seqs, n_sp * width), bf16),
        in_specs=[hbm, vmem] + [hbm] * (1 + count) + [vmem, vmem, hbm],
        out_specs=vmem,
        scratch_shapes=[
            pltpu.VMEM(tokens.shape, bf16),
            pltpu.VMEM(tokens.shape, jnp.float32),
            pltpu.VMEM(shift.shape, shift.dtype),
            pltpu.VMEM((n_sp, seqs, n_tp * span, KEY), bf16),
            pltpu.VMEM((seqs, length, KEY), bf16),
            pltpu.VMEM((seqs, length, model), bf16),
            pltpu.VMEM((model, count * KEY), bf16),
            pltpu.VMEM((seqs, length, count * KEY), bf16),
            pltpu.VMEM((seqs, length, VAL), jnp.float32),
            pltpu.VMEM((seqs, n_sp, n_x, CORES, span, VAL), bf16),
            pltpu.VMEM((n_x, seqs, span, CORES * depth), bf16),
            pltpu.VMEM((CORES * depth, n_sp * width), bf16),
            pltpu.VMEM((n_x, seqs, span, n_sp * width), bf16),
            pltpu.VMEM((seqs, span, n_sp * width), bf16),
            dma((2,)),
            dma((count + 1,)),
            dma((2, slots - 1, PIECES)),
            dma((2, slots, PIECES)),
            dma((2, 2, slots, PIECES)),
            dma((2, n_sp - 1, count)),
            dma((2, n_sp - 1, count)),
            dma((2, n_sp - 1)),
            dma((2, slots - 1)),
            dma((2, slots - 1)),
            dma((2, 2, slots)),
            dma((2, seqs, n_sp, CORES)),
            dma((2, PIECES, strips)),
        ],
        compiler_params=pltpu.CompilerParams(
            collective_id=0, has_side_effects=True, vmem_limit_bytes=56 * 1024 * 1024
        ),
    )(tokens, norm_gain, shift, *sources, gap, gain, w_out)


def head_shards(
    sizes,
    tokens,
    norm_gain,
    w_query,
    w_value,
    w_fwd_gate,
    w_bwd_gate,
    w_out_gate,
    floor_gap,
    decay_shift,
    head_gain,
    w_out,
):
    return layer(
        sizes,
        tokens,
        norm_gain.reshape(1, 1, -1),
        decay_shift,
        (w_query, w_value, w_fwd_gate, w_bwd_gate, w_out_gate),
        floor_gap,
        head_gain.reshape(1, VAL),
        w_out,
    )


def by_heads(mesh):
    n_sp, n_tp = mesh.shape["sp"], mesh.shape["tp"]

    def run(*arrays):
        tokens, w_query = arrays[0], arrays[2]
        heads_here = w_query.shape[1] // KEY // n_tp
        span = tokens.shape[0] // (n_sp * n_tp)
        sizes = (mesh.shape["grp"], n_sp, n_tp)
        fits = heads_here == n_sp and n_sp > 2 and n_tp == 2 * CORES and span % 16 == 0
        fits = fits and sizes[0] == 2 and tokens.shape[1] // sizes[0] % PIECES == 0
        fits = fits and tokens.shape[0] % BLOCK == 0 and tokens.shape[0] <= 512
        body = functools.partial(head_shards, sizes) if fits else shards
        return mapped(body, mesh)(*arrays)

    return run


def mapped(body, mesh):
    return jax.shard_map(
        body,
        mesh=mesh,
        in_specs=(
            P(("sp", "tp"), "grp", None),
            P(),
            P("sp", "tp"),
            P("sp", "tp"),
            P("sp", "tp"),
            P("sp", "tp"),
            P("sp", "tp"),
            P(None, "tp"),
            P("sp", "grp", "tp"),
            P(),
            P("tp", "sp"),
        ),
        out_specs=P(("sp", "tp"), "grp", None),
        check_vma=False,
    )


def solution(mesh):
    return by_heads(mesh)
```

time: 95.7 us -> 97.5 us (1.019)
  Pallas kernels: 90.7 us -> 95.2 us
  local copies, waits for them, and re-layouts: 4.56 us -> 1.76 us
    pallas_call x1, Pallas kernels: 90.7 us -> 95.2 us  [layer(): pl.pallas_call(functools.partial(layer_kernel, sizes), out_shape=jax.Shap...]
    transpose x1 -> x0, local copies, waits for them, and re-layouts: 1.86 us -> none  [head_shards(): return layer(sizes, tokens.transpose(1, 0, 2), norm_gain.reshape(1, 1, -1...]
    unnamed x4 -> x1, local copies, waits for them, and re-layouts: 2.7 us -> 1.76 us
where the time goes in v1:
time: 97.5 us; the launch traced here: 97 us
  Pallas kernels  95.2 us (98%)
  local copies, waits for them, and re-layouts  1.76 us (2%)
    pallas_call x1, Pallas kernels, layer(): pl.pallas_call(functools.partial(layer_kernel, sizes), out_shape=jax.Shap...  95.2 us

profile of v1, /device:TPU:0, one launch (start us, length us, event | category | flops | bytes accessed | tf_op | source)
XLA Modules:
  0.0 97.0 jit_solution(8781083187461626733)
XLA Ops:
  0.0 95.2 %shard_map.109 = bf16[16,4,2048]{2,1,0:T(4,128)(2,1)} custom-call(bf16[16,4,2048]{2,1,0:T(4,128)(2,1)} %token_ref.1, f32[1,1,2048]{2,1,0:T(1,128)} %bitcast.2, f32[64,4,512]{2,1,0:T(4,128)} %shift_ref.1, bf16[512,512]{1,0:T(8,128)(2,1)} %wq_ref.1, bf16[512,512]{1,0:T(8,128)(2,1)} %wv_ref.1, bf16[512,512]{1,0:T(8,128)(2,1)} %wf_ref.1, ...), custom_call_target="tpu_custom_call" | custom-call | tf_op jit(solution)/shard_map/pallas_call | solution.py:747
  95.2 1.8 %copy.13 = bf16[16,4,2048]{2,1,0:T(4,128)(2,1)} copy(bf16[16,4,2048]{2,1,0:T(4,128)(2,1)} %shard_map.109) | data formatting | bytes 524288

commit v2 on v1

--- a/solution.py
+++ b/solution.py
@@ -205,6 +205,7 @@
 MESH = pl.DeviceIdType.MESH
 CORES = 2
 PIECES = 2
+scope = jax.named_scope
 
 
 def recur_one(proj_ref, shift_ref, gap_ref, gain_ref, out_ref, i, own):
@@ -276,9 +277,11 @@
                 )
                 state[d] = fresh if state[d] is None else state[d] * jnp.exp(edge) + fresh
     for n in range(blocks):
-        combined = outs[n][0] + outs[n][1]
-        scale = lax.rsqrt(jnp.mean(combined * combined, axis=-1, keepdims=True) + norm_eps)
-        out_ref[i, n * BLOCK : (n + 1) * BLOCK] = combined * scale * gain_ref[...]
+        out_ref[n * BLOCK : (n + 1) * BLOCK] = outs[n][0] + outs[n][1]
+    combined = out_ref[...]
+    normed = combined * lax.rsqrt(jnp.mean(combined * combined, axis=-1, keepdims=True) + norm_eps)
+    gate = cols(4).astype(f32)
+    return (normed * gain_ref[...] * (gate * jax.nn.sigmoid(gate))).astype(bf16)
 
 
 def layer_kernel(
@@ -310,18 +313,28 @@
     partial,
     landed,
     load_sem,
-    own_sem,
-    az_sem,
-    ax_sem,
-    ac_sem,
-    wz_sem,
-    wy_sem,
-    sz_sem,
-    oz_sem,
-    oy_sem,
-    oc_sem,
-    m_sem,
-    p_sem,
+    az_out,
+    az_in,
+    ax_out,
+    ax_in,
+    ac_out,
+    ac_in,
+    wz_out,
+    wz_in,
+    wy_out,
+    wy_in,
+    sz_out,
+    sz_in,
+    oz_out,
+    oz_in,
+    oy_out,
+    oy_in,
+    oc_out,
+    oc_in,
+    m_out,
+    m_in,
+    p_out,
+    p_in,
 ):
     bf16 = jnp.bfloat16
     f32 = jnp.float32
@@ -341,26 +354,34 @@
     half = depth // n_grp
     width = w_ref.shape[1]
     lot = seqs // PIECES
+    bit = half // PIECES
     sources = (wq_ref, wv_ref, wf_ref, wb_ref, wg_ref)
     count = len(sources)
+    groups = ((0, 2), (2, 4), (4, 5))
     last = n_sp - 1
     z_at = [lax.rem(s + k, n_sp) for k in range(n_sp)]
     z_from = [lax.rem(s + n_sp - k, n_sp) for k in range(n_sp)]
     core_at = [c, 1 - c]
 
+    def span_at(where, size):
+        return pl.ds(pl.multiple_of(where * size, size), size)
+
     def lanes(where, size=KEY):
-        return pl.ds(pl.multiple_of(where * size, size), size)
-
-    def remote(src, dst, sems, index, peer):
+        return span_at(where, size)
+
+    def remote(src, dst, out_sem, in_sem, peer):
         return pltpu.make_async_remote_copy(
             src_ref=src,
             dst_ref=dst,
-            send_sem=sems.at[(0, *index)],
-            recv_sem=sems.at[(1, *index)],
+            send_sem=out_sem,
+            recv_sem=in_sem,
             device_id=peer,
             device_id_type=MESH,
         )
 
+    def tally(ref, out_sem, in_sem):
+        return remote(ref, ref, out_sem, in_sem, (g, s, twin))
+
     def inside(place):
         return jnp.logical_and(place >= 0, place < n_sp)
 
@@ -369,6 +390,9 @@
 
     def slot(up, d):
         return 1 + d if up else n_sp + d
+
+    def end(up):
+        return 0 if up else last
 
     def sends(up, d):
         return jnp.logical_and(inside(s + step_of(up)), inside(s - step_of(up) * d))
@@ -382,13 +406,6 @@
             @pl.when(gets(up, d))
             def _():
                 visit(up, d, s - step_of(up) * (d + 1))
-
-    sent = []
-
-    def go(copy):
-        copy.start()
-        sent.append(copy)
-        return copy
 
     load_rows = pltpu.make_async_copy(token_ref, rows_in, load_sem.at[0])
     load_shift = pltpu.make_async_copy(shift_ref, raw_shift, load_sem.at[1])
@@ -399,44 +416,121 @@
     barrier = pltpu.get_barrier_semaphore()
     for peer in peers:
         pl.semaphore_signal(barrier, inc=1, device_id=peer, device_id_type=MESH)
-    mine = [
+    own_rows = span_at(s, depth)
+    for p, w in enumerate(sources):
         pltpu.make_async_copy(
-            w.at[:, lanes(s)],
-            weights.at[pl.ds(pl.multiple_of(s * depth, depth), depth), pl.ds(p * KEY, KEY)],
-            own_sem.at[p],
-        )
-        for p, w in enumerate(sources)
-    ]
-    w_rows = pl.ds(pl.multiple_of(c * depth, depth), depth)
-    w_own = pltpu.make_async_copy(w_ref, matrix.at[w_rows, lanes(s, width)], own_sem.at[count])
-    for copy in mine:
-        copy.start()
+            w.at[:, lanes(s)], weights.at[own_rows, pl.ds(p * KEY, KEY)], load_sem.at[2]
+        ).start()
+    w_rows = span_at(c, depth)
+    w_own = pltpu.make_async_copy(w_ref, matrix.at[w_rows, lanes(s, width)], load_sem.at[3])
     w_own.start()
 
-    here_rows = pl.ds(pl.multiple_of((s * n_tp + t) * span, span), span)
-    load_rows.wait()
+    here_rows = span_at(s * n_tp + t, span)
+    with scope("wait_rows"):
+        load_rows.wait()
     rows = rows_in[...].astype(f32)
     scale = lax.rsqrt(jnp.mean(rows * rows, axis=-1, keepdims=True) + norm_eps)
     wide[...] = rows * scale * norm_ref[...]
     for q in range(seqs):
         acts[q, here_rows, :] = wide[:, q, :].astype(bf16)
-    pl.semaphore_wait(barrier, len(peers))
-
-    def block(where_s, where_t, piece):
-        at = pl.ds(pl.multiple_of((where_s * n_tp + where_t) * span, span), span)
-        return acts.at[pl.ds(piece * lot, lot), at, :]
+    with scope("barrier"):
+        pl.semaphore_wait(barrier, len(peers))
+
+    def block(where_s, where_t):
+        return acts.at[:, span_at(where_s * n_tp + where_t, span), :]
 
     def act_z(up, d, piece):
-        here = block(s - step_of(up) * d, t, piece)
-        return remote(here, here, az_sem, (slot(up, d) - 1, piece), (g, s + step_of(up), t))
-
-    def act_x(index, origin, piece):
-        here = block(origin, t, piece)
-        return remote(here, here, ax_sem, (index, piece), (g, s, across))
-
-    def act_c(far, index, origin, piece):
-        here = block(origin, across if far else t, piece)
-        return remote(here, here, ac_sem, (far, index, piece), (g, s, twin))
+        at = span_at((s - step_of(up) * d) * n_tp + t, span)
+        here = acts.at[pl.ds(piece * lot, lot), at, :]
+        index = slot(up, d) - 1
+        peer = (g, s + step_of(up), t)
+        return remote(here, here, az_out.at[index], az_in.at[index, piece], peer)
+
+    def act_x(index, origin):
+        here = block(origin, t)
+        return remote(here, here, ax_out, ax_in.at[index], (g, s, across))
+
+    def act_c(far, origin):
+        here = block(origin, across if far else t)
+        return remote(here, here, ac_out, ac_in, (g, s, twin))
+
+    part = span_at(g, half)
+
+    def w_cols(group):
+        first, stop = groups[group]
+        return pl.ds(first * KEY, (stop - first) * KEY)
+
+    def w_z(k, group, p):
+        src = sources[p].at[part, lanes(z_at[k])]
+        dst = weights.at[span_at(s * n_grp + g, half), pl.ds(p * KEY, KEY)]
+        return remote(src, dst, wz_out, wz_in.at[k - 1, group], (g, z_at[k], t))
+
+    def w_block(k, group):
+        return weights.at[span_at(z_from[k] * n_grp + g, half), w_cols(group)]
+
+    def w_y(k, group):
+        here = w_block(k, group)
+        return remote(here, here, wy_out, wy_in.at[group], (1 - g, s, t))
+
+    place = span_at(s, positions)
+
+    def s_z(k):
+        return remote(own_shift.at[z_at[k]], shifts.at[:, place, :], sz_out, sz_in, (g, z_at[k], t))
+
+    def o_block(where_s, where_g, where_c, piece):
+        at = pl.multiple_of(where_c * depth + where_g * half + piece * bit, bit)
+        return matrix.at[pl.ds(at, bit), lanes(where_s, width)]
+
+    def o_z(up, d, piece):
+        here = o_block(s - step_of(up) * d, g, c, piece)
+        src = w_ref.at[span_at(g * PIECES + piece, bit), :] if d == 0 else here
+        index = slot(up, d) - 1
+        peer = (g, s + step_of(up), t)
+        return remote(src, here, oz_out.at[index], oz_in.at[index, piece], peer)
+
+    def o_y(index, origin, piece):
+        here = o_block(origin, g, c, piece)
+        return remote(here, here, oy_out, oy_in.at[index - 1, piece], (1 - g, s, t))
+
+    def o_c(far, index, origin, piece):
+        here = o_block(origin, 1 - g if far else g, c, piece)
+        return remote(here, here, oc_out, oc_in.at[index], (g, s, twin))
+
+    def ahead(up, groups_now):
+        for hop in range(1, n_sp):
+            k = hop if up else n_sp - hop
+            go_up = s + k < n_sp
+
+            @pl.when(go_up if up else jnp.logical_not(go_up))
+            def _():
+                for group in groups_now:
+                    if group is None:
+                        s_z(k).start()
+                    else:
+                        for p in range(*groups[group]):
+                            w_z(k, group, p).start()
+
+    def o_first(up):
+        @pl.when(sends(up, 0))
+        def _():
+            for piece in range(PIECES):
+                o_z(up, 0, piece).start()
+
+    def issue(up):
+        pl.when(s == end(up))(lambda: o_first(up))
+        ahead(up, range(len(groups)))
+
+        @pl.when(s != end(up))
+        def _():
+            ahead(up, (None,))
+            o_first(up)
+
+    def issue_rest():
+        for up in (True, False):
+
+            @pl.when(s == end(up))
+            def _():
+                ahead(up, (None,))
 
     for piece in range(PIECES):
         for up in (True, False):
@@ -445,83 +539,18 @@
             def _():
                 act_z(up, 0, piece).start()
 
-        act_x(0, s, piece).start()
-    for piece in range(PIECES):
-        act_c(0, 0, s, piece).start()
-
-    load_shift.wait()
+    act_x(0, s).start()
+    act_c(0, s).start()
+    with scope("wait_shift_load"):
+        load_shift.wait()
     for q in range(seqs):
         values = raw_shift[:, q, :].astype(bf16)
         for k in range(n_sp):
             own_shift[k, q] = values[:, k * KEY : (k + 1) * KEY]
-    place = pl.ds(pl.multiple_of(s * positions, positions), positions)
     shifts[:, place, :] = own_shift[s]
-
-    part = pl.ds(pl.multiple_of(g * half, half), half)
-
-    def w_rows_of(where_s, where_g):
-        return pl.ds(pl.multiple_of(where_s * depth + where_g * half, half), half)
-
-    def w_z(k, p):
-        return remote(
-            sources[p].at[part, lanes(z_at[k])],
-            weights.at[w_rows_of(s, g), pl.ds(p * KEY, KEY)],
-            wz_sem,
-            (k - 1, p),
-            (g, z_at[k], t),
-        )
-
-    def w_y(k, p):
-        here = weights.at[w_rows_of(z_from[k], g), pl.ds(p * KEY, KEY)]
-        return remote(here, here, wy_sem, (k - 1, p), (1 - g, s, t))
-
-    def s_z(k):
-        return remote(own_shift.at[z_at[k]], shifts.at[:, place, :], sz_sem, (k - 1,), (g, z_at[k], t))
-
-    def o_block(where_s, where_g, where_c):
-        at = pl.ds(pl.multiple_of(where_c * depth + where_g * half, half), half)
-        return matrix.at[at, lanes(where_s, width)]
-
-    def o_z(up, d):
-        origin = s - step_of(up) * d
-        here = o_block(origin, g, c)
-        src = w_ref.at[part, :] if d == 0 else here
-        return remote(src, here, oz_sem, (slot(up, d) - 1,), (g, s + step_of(up), t))
-
-    def o_y(index, origin):
-        here = o_block(origin, g, c)
-        return remote(here, here, oy_sem, (index - 1,), (1 - g, s, t))
-
-    def o_c(far, index, origin):
-        here = o_block(origin, 1 - g if far else g, c)
-        return remote(here, here, oc_sem, (far, index), (g, s, twin))
-
-    def o_own():
-        at = matrix.at[w_rows, lanes(s, width)]
-        return remote(w_ref, at, oc_sem, (0, 0), (g, s, twin))
-
-    def issue(up):
-        def ahead(visit):
-            for k in range(1, n_sp):
-                go_up = s + k < n_sp
-
-                @pl.when(go_up if up else jnp.logical_not(go_up))
-                def _():
-                    visit(k)
-
-        for p in range(count - 1):
-            ahead(lambda k: w_z(k, p).start())
-        ahead(lambda k: s_z(k).start())
-
-        @pl.when(sends(up, 0))
-        def _():
-            o_z(up, 0).start()
-
-        ahead(lambda k: w_z(k, count - 1).start())
-
     for up in (True, False):
 
-        @pl.when(s == (0 if up else last))
+        @pl.when(s == end(up))
         def _():
             issue(up)
 
@@ -536,10 +565,12 @@
                     def _():
                         act_z(up, d + 1, piece).start()
 
-                act_x(slot(up, d), origin, piece).start()
-                act_c(0, slot(up, d), origin, piece).start()
-
-            each(d, arrived)
+                if piece == PIECES - 1:
+                    act_x(slot(up, d), origin).start()
+                    act_c(0, origin).start()
+
+            with scope(f"act_z{d}_{piece}"):
+                each(d, arrived)
         if d + 1 < last:
             for up in (True, False):
 
@@ -547,40 +578,69 @@
                 def _():
                     issue(up)
 
-    o_own().start()
+    o_own = remote(w_ref, matrix.at[w_rows, lanes(s, width)], oc_out, oc_in.at[0], (g, s, twin))
+    o_own.start()
 
     def relay(index, origin):
+        act_x(index, origin).wait_recv()
+        act_c(1, origin).start()
+
+    def swap(up, d, origin):
+        k = d + 1 if up else last - d
+        for group in range(len(groups)):
+            tally(w_block(k, group), wz_out, wz_in.at[k - 1, group]).wait_recv()
+            w_y(k, group).start()
+
+    def o_take(up, d, origin):
         for piece in range(PIECES):
-            act_x(index, origin, piece).wait_recv()
-            act_c(1, index, origin, piece).start()
-
-    def swap(p):
-        for k in range(1, n_sp):
-            w_z(k, p).wait_recv()
-            go(w_y(k, p))
-
-    relay(0, s)
-    for d in range(last):
-        each(d, lambda up, d, origin: relay(slot(up, d), origin))
-        if d < 2:
-            swap(d)
-
-    def joined(index, origin):
+            o_z(up, d, piece).wait_recv()
+            if d + 1 < last:
+
+                @pl.when(sends(up, d + 1))
+                def _():
+                    o_z(up, d + 1, piece).start()
+
+            o_y(slot(up, d), origin, piece).start()
+            o_c(0, slot(up, d), origin, piece).start()
+
+    def take_early(up):
         for piece in range(PIECES):
-            for far in range(2):
-                act_c(far, index, origin, piece).wait_recv()
-
-    joined(0, s)
-    for d in range(last):
-        each(d, lambda up, d, origin: joined(slot(up, d), origin))
-    for copy in mine:
-        copy.wait()
-
-    def project(first, end):
-        for p in range(first, end):
-            for k in range(1, n_sp):
-                w_y(k, p).wait_recv()
-        at = slice(first * KEY, end * KEY)
+            o_z(up, 0, piece).wait_recv()
+            o_y(slot(up, 0), s - step_of(up), piece).start()
+            o_c(0, slot(up, 0), s - step_of(up), piece).start()
+
+    def o_swapped(up, d, origin):
+        for piece in range(PIECES):
+            o_y(slot(up, d), origin, piece).wait_recv()
+            o_c(1, slot(up, d), origin, piece).start()
+
+    def neighbour(up):
+        return s == (1 if up else last - 1)
+
+    with scope("take_early"):
+        for up in (True, False):
+            pl.when(neighbour(up))(lambda: take_early(up))
+    with scope("swap_near"):
+        each(0, swap)
+    with scope("relay"):
+        relay(0, s)
+        for d in range(last):
+            each(d, lambda up, d, origin: relay(slot(up, d), origin))
+    for d in range(last - 1, 0, -1):
+        with scope(f"swap_far{d}"):
+            each(d, swap)
+    issue_rest()
+
+    with scope("joined"):
+        tally(acts.at[pl.ds(0, seqs // CORES)], ac_out, ac_in).wait_recv()
+        here = weights.at[own_rows, :]
+        pltpu.make_async_copy(here, here, load_sem.at[2]).wait()
+
+    def project(group):
+        with scope(f"wait_w{group}"):
+            block = weights.at[pl.ds(0, last * half), w_cols(group)]
+            tally(block, wy_out, wy_in.at[group]).wait_recv()
+        at = slice(groups[group][0] * KEY, groups[group][1] * KEY)
 
         def one(q, carry):
             proj[q, :, at] = jnp.dot(
@@ -588,40 +648,25 @@
             ).astype(bf16)
             return carry
 
-        lax.fori_loop(0, seqs, one, 0)
-
-    def o_arrived(up, d, origin):
-        o_z(up, d).wait_recv()
-        if d + 1 < last:
-
-            @pl.when(sends(up, d + 1))
-            def _():
-                o_z(up, d + 1).start()
-
-        o_y(slot(up, d), origin).start()
-        o_c(0, slot(up, d), origin).start()
-
-    def o_swapped(up, d, origin):
-        o_y(slot(up, d), origin).wait_recv()
-        o_c(1, slot(up, d), origin).start()
-
-    def recur(q, carry):
-        recur_one(proj, shifts, gap_ref, gain_ref, summed, q, lanes(s))
-        return carry
-
-    swap(2)
-    project(0, 2)
-    swap(3)
-    project(2, 4)
-    for k in range(1, n_sp):
-        s_z(k).wait_recv()
-    lax.fori_loop(0, seqs // 2, recur, 0)
-    each(0, o_arrived)
-    swap(4)
-    lax.fori_loop(seqs // 2, seqs, recur, 0)
-    each(1, o_arrived)
-    each(0, o_swapped)
-    project(4, 5)
+        with scope(f"project{group}"):
+            lax.fori_loop(0, seqs, one, 0)
+
+    project(0)
+    with scope("act_drain"):
+        tally(acts.at[:, pl.ds(0, n_sp * span), :], ax_out, ax_in.at[0]).wait_send()
+        tally(acts.at[pl.ds(0, seqs // CORES)], ac_out, ac_in).wait_send()
+        for d in range(last):
+            for up in (True, False):
+
+                @pl.when(sends(up, d))
+                def _():
+                    index = slot(up, d) - 1
+                    tally(block(s, t), az_out.at[index], az_in.at[index, 0]).wait_send()
+
+    project(1)
+    project(2)
+    with scope("wait_shift"):
+        tally(shifts.at[:, pl.ds(0, last * positions), :], sz_out, sz_in).wait_recv()
 
     targets = [(k, o) for k in range(n_sp) for o in range(CORES) if k or o]
 
@@ -629,106 +674,104 @@
         return remote(
             mixed.at[q, z_at[k], :, core_at[o]],
             heads.at[:, q, :, lanes(c * n_sp + s, VAL)],
-            m_sem,
-            (q, k, o),
+            m_out,
+            m_in,
             (g, z_at[k], x * CORES + core_at[o]),
         )
 
-    def mix(q, carry):
-        gate = proj[q, :, 4 * KEY : 5 * KEY].astype(f32)
-        value = (summed[q] * (gate * jax.nn.sigmoid(gate))).astype(bf16)
+    def recur(q, carry):
+        value = recur_one(proj, shifts, gap_ref, gain_ref, summed, q, lanes(s))
         mixed[q] = value.reshape(n_sp, n_x, CORES, span, VAL)
         heads[:, q, :, lanes(c * n_sp + s, VAL)] = mixed[q, s, :, c]
         for k, o in targets:
             m_move(q, k, o).start()
         return carry
 
-    lax.fori_loop(0, seqs, mix, 0)
-    for d in range(2, last):
-        each(d, o_arrived)
+    with scope("recur"):
+        lax.fori_loop(0, seqs, recur, 0)
+    with scope("forward"):
+        for up in (True, False):
+
+            @pl.when(jnp.logical_and(neighbour(up), sends(up, 1)))
+            def _():
+                for piece in range(PIECES):
+                    o_z(up, 1, piece).start()
+
+    with scope("take_late"):
+        for up in (True, False):
+
+            @pl.when(jnp.logical_and(gets(up, 0), jnp.logical_not(neighbour(up))))
+            def _():
+                o_take(up, 0, s - step_of(up))
+
+    with scope("w_drain"):
+        tally(own_shift.at[pl.ds(0, last)], sz_out, sz_in).wait_send()
+        every = weights.at[pl.ds(0, last * half), :]
+        tally(every, wz_out, wz_in.at[0, 0]).wait_send()
+        tally(every, wy_out, wy_in.at[0]).wait_send()
     for d in range(1, last):
-        each(d, o_swapped)
+        with scope(f"o_swapped{d - 1}"):
+            each(d - 1, o_swapped)
+        with scope(f"o_pass{d}"):
+            each(d, o_take)
     w_own.wait()
-    o_own().wait_recv()
-
-    def o_joined(up, d, origin):
-        for far in range(2):
-            o_c(far, slot(up, d), origin).wait_recv()
-
-    for d in range(last):
-        each(d, o_joined)
-
-    strips = matrix.shape[1] // width
-
-    def p_move(h, n):
-        both = pl.ds(h * lot, lot)
-        at = pl.ds(n * width, width)
-        return remote(
-            partial.at[1 - x, both, :, at],
-            landed.at[both, :, at],
-            p_sem,
-            (h, n),
-            (g, s, across),
+
+    def p_move(index, origin):
+        at = lanes(origin, width)
+        peer = (g, s, across)
+        return remote(partial.at[1 - x, :, :, at], landed.at[:, :, at], p_out, p_in.at[index], peer)
+
+    def strip(index, origin):
+        at = lanes(origin, width)
+        tally(matrix.at[pl.ds(0, depth), at], oc_out, oc_in.at[index]).wait_recv()
+        lines = heads[...].reshape(n_x * seqs * span, -1)
+        partial[:, :, :, at] = (
+            jnp.dot(lines, matrix[:, at], preferred_element_type=f32)
+            .astype(bf16)
+            .reshape(n_x, seqs, span, width)
         )
-
-    for h in range(PIECES):
-        both = slice(h * lot, (h + 1) * lot)
-        for q in range(h * lot, (h + 1) * lot):
-            for k, o in targets:
-                m_move(q, k, o).wait_recv()
-        lines = heads[:, both].reshape(n_x * lot * span, -1)
-        for n in range(strips):
-            at = slice(n * width, (n + 1) * width)
-            partial[:, both, :, at] = (
-                jnp.dot(lines, matrix[:, at], preferred_element_type=f32)
-                .astype(bf16)
-                .reshape(n_x, lot, span, width)
-            )
-            go(p_move(h, n))
-    for h in range(PIECES):
-        for n in range(strips):
-            p_move(h, n).wait_recv()
-        for q in range(h * lot, (h + 1) * lot):
-            wide[:, q, :] = partial[x, q].astype(f32) + landed[q].astype(f32)
-    out_ref[...] = wide[...].astype(bf16)
-
-    for copy in sent:
-        copy.wait_send()
-    for k in range(1, n_sp):
-        s_z(k).wait_send()
-        for p in range(count):
-            w_z(k, p).wait_send()
-    o_own().wait_send()
-    for piece in range(PIECES):
-        act_x(0, s, piece).wait_send()
-        for far in range(2):
-            act_c(far, 0, s, piece).wait_send()
-    for d in range(last):
-        for up in (True, False):
-
-            @pl.when(sends(up, d))
-            def _():
-                o_z(up, d).wait_send()
-                for piece in range(PIECES):
-                    act_z(up, d, piece).wait_send()
-
-        def gone(up, d, origin):
-            o_y(slot(up, d), origin).wait_send()
-            for far in range(2):
-                o_c(far, slot(up, d), origin).wait_send()
-            for piece in range(PIECES):
-                act_x(slot(up, d), origin, piece).wait_send()
-                for far in range(2):
-                    act_c(far, slot(up, d), origin, piece).wait_send()
-
-        each(d, gone)
-
-    def drain(q, carry):
-        for k, o in targets:
-            m_move(q, k, o).wait_send()
-        return carry
-
-    lax.fori_loop(0, seqs, drain, 0)
+        p_move(index, origin).start()
+
+    def o_strip(up, d, origin):
+        strip(slot(up, d), origin)
+
+    all_mixed = tally(heads.at[:, :, :, pl.ds(0, len(targets) * VAL)], m_out, m_in)
+    with scope("wait_m"):
+        all_mixed.wait_recv()
+    with scope("own_strip"):
+        strip(0, s)
+    for d in range(last - 1):
+        with scope(f"strip{d}"):
+            each(d, o_strip)
+    with scope(f"o_swapped{last - 1}"):
+        each(last - 1, o_swapped)
+    with scope(f"strip{last - 1}"):
+        each(last - 1, o_strip)
+
+    def finish(index, origin):
+        p_move(index, origin).wait_recv()
+        at = lanes(origin, width)
+        total = partial[x, :, :, at].astype(f32) + landed[:, :, at].astype(f32)
+        out_ref[:, :, at] = total.astype(bf16)
+
+    with scope("finish"):
+        finish(0, s)
+        for d in range(last):
+            each(d, lambda up, d, origin: finish(slot(up, d), origin))
+    with scope("drain"):
+        all_mixed.wait_send()
+        strips = matrix.at[pl.ds(0, half), pl.ds(0, last * width)]
+        tally(strips, oy_out, oy_in.at[0, 0]).wait_send()
+        tally(matrix.at[pl.ds(0, depth), :], oc_out, oc_in.at[0]).wait_send()
+        tally(landed, p_out, p_in.at[0]).wait_send()
+        for d in range(last):
+            for up in (True, False):
+
+                @pl.when(sends(up, d))
+                def _():
+                    index = slot(up, d) - 1
+                    here = matrix.at[pl.ds(0, half), pl.ds(0, width)]
+                    tally(here, oz_out.at[index], oz_in.at[index, 0]).wait_send()
 
 
 def layer(sizes, tokens, norm_gain, shift, sources, gap, gain, w_out):
@@ -739,14 +782,13 @@
     count = len(sources)
     depth, width = w_out.shape
     slots = 2 * n_sp - 1
-    strips = n_sp
     dma = pltpu.SemaphoreType.DMA
     hbm = pl.BlockSpec(memory_space=pltpu.HBM)
     vmem = pl.BlockSpec(memory_space=pltpu.VMEM)
     bf16 = jnp.bfloat16
     return pl.pallas_call(
         functools.partial(layer_kernel, sizes),
-        out_shape=jax.ShapeDtypeStruct((span, seqs, n_sp * width), bf16),
+        out_shape=jax.ShapeDtypeStruct((seqs, span, n_sp * width), bf16),
         in_specs=[hbm, vmem] + [hbm] * (1 + count) + [vmem, vmem, hbm],
         out_specs=vmem,
         scratch_shapes=[
@@ -758,25 +800,35 @@
             pltpu.VMEM((seqs, length, model), bf16),
             pltpu.VMEM((model, count * KEY), bf16),
             pltpu.VMEM((seqs, length, count * KEY), bf16),
-            pltpu.VMEM((seqs, length, VAL), jnp.float32),
+            pltpu.VMEM((length, VAL), jnp.float32),
             pltpu.VMEM((seqs, n_sp, n_x, CORES, span, VAL), bf16),
             pltpu.VMEM((n_x, seqs, span, CORES * depth), bf16),
             pltpu.VMEM((CORES * depth, n_sp * width), bf16),
             pltpu.VMEM((n_x, seqs, span, n_sp * width), bf16),
             pltpu.VMEM((seqs, span, n_sp * width), bf16),
-            dma((2,)),
-            dma((count + 1,)),
-            dma((2, slots - 1, PIECES)),
-            dma((2, slots, PIECES)),
-            dma((2, 2, slots, PIECES)),
-            dma((2, n_sp - 1, count)),
-            dma((2, n_sp - 1, count)),
-            dma((2, n_sp - 1)),
-            dma((2, slots - 1)),
-            dma((2, slots - 1)),
-            dma((2, 2, slots)),
-            dma((2, seqs, n_sp, CORES)),
-            dma((2, PIECES, strips)),
+            dma((4,)),
+            dma((slots - 1,)),
+            dma((slots - 1, PIECES)),
+            dma,
+            dma((slots,)),
+            dma,
+            dma,
+            dma,
+            dma((n_sp - 1, 3)),
+            dma,
+            dma((3,)),
+            dma,
+            dma,
+            dma((slots - 1,)),
+            dma((slots - 1, PIECES)),
+            dma,
+            dma((slots - 1, PIECES)),
+            dma,
+            dma((slots,)),
+            dma,
+            dma,
+            dma,
+            dma((slots,)),
         ],
         compiler_params=pltpu.CompilerParams(
             collective_id=0, has_side_effects=True, vmem_limit_bytes=56 * 1024 * 1024
@@ -807,7 +859,7 @@
         floor_gap,
         head_gain.reshape(1, VAL),
         w_out,
-    )
+    ).transpose(1, 0, 2)
 
 
 def by_heads(mesh):

time: 97.5 us -> 87.1 us (0.89)
  Pallas kernels: 95.2 us -> 85 us
    pallas_call x1, Pallas kernels: 95.2 us -> 85 us  [layer(): pl.pallas_call(functools.partial(layer_kernel, sizes), out_shape=jax.Shap...]
    transpose x0 -> x1, local copies, waits for them, and re-layouts: none -> 1.86 us  [head_shards(): return layer(sizes, tokens, norm_gain.reshape(1, 1, -1), decay_shift, (w_...]
    unnamed x1 -> x0, local copies, waits for them, and re-layouts: 1.76 us -> none
where the time goes in v2:
time: 87.1 us; the launch traced here: 86.9 us
  Pallas kernels  85 us (98%)
  local copies, waits for them, and re-layouts  1.86 us (2%)
    pallas_call x1, Pallas kernels, layer(): pl.pallas_call(functools.partial(layer_kernel, sizes), out_shape=jax.Shap...  85 us
    transpose x1, local copies, waits for them, and re-layouts, head_shards(): return layer(sizes, tokens, norm_gain.reshape(1, 1, -1), decay_shift, (w_...  1.86 us

profile of v2, /device:TPU:0, one launch (start us, length us, event | category | flops | bytes accessed | tf_op | source)
XLA Modules:
  0.0 86.9 jit_solution(2769556043258723921)
XLA Ops:
  0.0 85.0 %shard_map.109 = bf16[4,16,2048]{2,1,0:T(8,128)(2,1)} custom-call(bf16[16,4,2048]{2,1,0:T(4,128)(2,1)} %token_ref.1, f32[1,1,2048]{2,1,0:T(1,128)} %bitcast.4, f32[64,4,512]{2,1,0:T(4,128)} %shift_ref.1, bf16[512,512]{1,0:T(8,128)(2,1)} %wq_ref.1, bf16[512,512]{1,0:T(8,128)(2,1)} %wv_ref.1, bf16[512,512]{1,0:T(8,128)(2,1)} %wf_ref.1, ...), custom_call_target="tpu_custom_call" | custom-call | tf_op jit(solution)/shard_map/pallas_call | solution.py:789
  85.1 1.9 %copy.12 = bf16[16,4,2048]{2,1,0:T(4,128)(2,1)} copy(bf16[16,4,2048]{2,0,1:T(8,128)(2,1)} %bitcast.3) | data formatting | bytes 524288 | tf_op jit(solution)/shard_map/transpose | solution.py:862

commit v3 on v2

--- a/solution.py
+++ b/solution.py
@@ -205,6 +205,9 @@
 MESH = pl.DeviceIdType.MESH
 CORES = 2
 PIECES = 2
+BITS = 4
+EARLY = 2
+HOLD = 5
 scope = jax.named_scope
 
 
@@ -305,6 +308,7 @@
     shifts,
     acts,
     weights,
+    begun,
     proj,
     summed,
     mixed,
@@ -354,7 +358,7 @@
     half = depth // n_grp
     width = w_ref.shape[1]
     lot = seqs // PIECES
-    bit = half // PIECES
+    bit = half // BITS
     sources = (wq_ref, wv_ref, wf_ref, wb_ref, wg_ref)
     count = len(sources)
     groups = ((0, 2), (2, 4), (4, 5))
@@ -456,21 +460,17 @@
 
     part = span_at(g, half)
 
-    def w_cols(group):
-        first, stop = groups[group]
-        return pl.ds(first * KEY, (stop - first) * KEY)
-
-    def w_z(k, group, p):
+    def w_z(k, p):
         src = sources[p].at[part, lanes(z_at[k])]
         dst = weights.at[span_at(s * n_grp + g, half), pl.ds(p * KEY, KEY)]
-        return remote(src, dst, wz_out, wz_in.at[k - 1, group], (g, z_at[k], t))
-
-    def w_block(k, group):
-        return weights.at[span_at(z_from[k] * n_grp + g, half), w_cols(group)]
-
-    def w_y(k, group):
-        here = w_block(k, group)
-        return remote(here, here, wy_out, wy_in.at[group], (1 - g, s, t))
+        return remote(src, dst, wz_out, wz_in.at[k - 1, p], (g, z_at[k], t))
+
+    def w_block(k, p):
+        return weights.at[span_at(z_from[k] * n_grp + g, half), pl.ds(p * KEY, KEY)]
+
+    def w_y(k, p, index):
+        here = w_block(k, p)
+        return remote(here, here, wy_out, wy_in.at[index], (1 - g, s, t))
 
     place = span_at(s, positions)
 
@@ -483,7 +483,7 @@
 
     def o_z(up, d, piece):
         here = o_block(s - step_of(up) * d, g, c, piece)
-        src = w_ref.at[span_at(g * PIECES + piece, bit), :] if d == 0 else here
+        src = w_ref.at[span_at(g * BITS + piece, bit), :] if d == 0 else here
         index = slot(up, d) - 1
         peer = (g, s + step_of(up), t)
         return remote(src, here, oz_out.at[index], oz_in.at[index, piece], peer)
@@ -496,8 +496,8 @@
         here = o_block(origin, 1 - g if far else g, c, piece)
         return remote(here, here, oc_out, oc_in.at[index], (g, s, twin))
 
-    def ahead(up, groups_now):
-        for hop in range(1, n_sp):
+    def ahead(up, hops, groups_now):
+        for hop in hops:
             k = hop if up else n_sp - hop
             go_up = s + k < n_sp
 
@@ -508,29 +508,46 @@
                         s_z(k).start()
                     else:
                         for p in range(*groups[group]):
-                            w_z(k, group, p).start()
-
-    def o_first(up):
+                            w_z(k, p).start()
+
+    every_group = range(len(groups))
+    every_hop = range(1, n_sp)
+
+    def neighbour(up):
+        return s == (1 if up else last - 1)
+
+    def o_first(up, pieces):
         @pl.when(sends(up, 0))
         def _():
-            for piece in range(PIECES):
+            for piece in pieces:
                 o_z(up, 0, piece).start()
 
     def issue(up):
-        pl.when(s == end(up))(lambda: o_first(up))
-        ahead(up, range(len(groups)))
-
-        @pl.when(s != end(up))
+        @pl.when(s == end(up))
         def _():
-            ahead(up, (None,))
-            o_first(up)
-
-    def issue_rest():
+            o_first(up, range(BITS))
+            ahead(up, (1,), every_group)
+
+        @pl.when(neighbour(not up))
+        def _():
+            ahead(up, every_hop[::-1], every_group)
+            o_first(up, range(BITS))
+            ahead(up, every_hop, (None,))
+
+        @pl.when(neighbour(up))
+        def _():
+            ahead(up, every_hop[::-1], every_group)
+            o_first(up, range(EARLY))
+            ahead(up, every_hop, (None,))
+            o_first(up, range(EARLY, BITS))
+
+    def issue_far():
         for up in (True, False):
 
             @pl.when(s == end(up))
             def _():
-                ahead(up, (None,))
+                ahead(up, every_hop[1:], every_group)
+                ahead(up, every_hop, (None,))
 
     for piece in range(PIECES):
         for up in (True, False):
@@ -554,7 +571,29 @@
         def _():
             issue(up)
 
+    def swap(d, groups_now, match=True, late=False):
+        for up in (True, False):
+
+            @pl.when(jnp.logical_and(gets(up, d), match))
+            def _():
+                k = d + 1 if up else last - d
+                for group in groups_now:
+                    for p in range(*groups[group]):
+                        tally(w_block(k, p), wz_out, wz_in.at[k - 1, p]).wait_recv()
+                        w_y(k, p, 1 + group if late else 0).start()
+
+    at_end = jnp.logical_or(s == 0, s == last)
+    late_source = jnp.where(at_end, last - s, lax.rem(s + 2, n_sp))
+
+    def swap_late(group):
+        swap(last - 1, (group,), at_end, True)
+        swap(last - 2, (group,), jnp.logical_not(at_end), True)
+
     for d in range(last):
+        if d == last - 1:
+            with scope("swap_end"):
+                for hop in range(last - 2, 0, -1):
+                    swap(hop, every_group, at_end)
         for piece in range(PIECES):
 
             def arrived(up, d, origin):
@@ -585,14 +624,8 @@
         act_x(index, origin).wait_recv()
         act_c(1, origin).start()
 
-    def swap(up, d, origin):
-        k = d + 1 if up else last - d
-        for group in range(len(groups)):
-            tally(w_block(k, group), wz_out, wz_in.at[k - 1, group]).wait_recv()
-            w_y(k, group).start()
-
-    def o_take(up, d, origin):
-        for piece in range(PIECES):
+    def o_take(up, d, origin, pieces=range(BITS)):
+        for piece in pieces:
             o_z(up, d, piece).wait_recv()
             if d + 1 < last:
 
@@ -603,55 +636,79 @@
             o_y(slot(up, d), origin, piece).start()
             o_c(0, slot(up, d), origin, piece).start()
 
-    def take_early(up):
-        for piece in range(PIECES):
-            o_z(up, 0, piece).wait_recv()
-            o_y(slot(up, 0), s - step_of(up), piece).start()
-            o_c(0, slot(up, 0), s - step_of(up), piece).start()
-
     def o_swapped(up, d, origin):
-        for piece in range(PIECES):
+        for piece in range(BITS):
             o_y(slot(up, d), origin, piece).wait_recv()
             o_c(1, slot(up, d), origin, piece).start()
 
-    def neighbour(up):
-        return s == (1 if up else last - 1)
-
     with scope("take_early"):
         for up in (True, False):
-            pl.when(neighbour(up))(lambda: take_early(up))
-    with scope("swap_near"):
-        each(0, swap)
+
+            @pl.when(neighbour(up))
+            def _():
+                o_take(up, 0, s - step_of(up))
+
+    with scope("swap_near0"):
+        swap(0, every_group[:1])
+    issue_far()
+    with scope("swap_near1"):
+        swap(0, every_group[1:])
     with scope("relay"):
         relay(0, s)
         for d in range(last):
             each(d, lambda up, d, origin: relay(slot(up, d), origin))
-    for d in range(last - 1, 0, -1):
-        with scope(f"swap_far{d}"):
-            each(d, swap)
-    issue_rest()
+
+    def take_late(pieces, where):
+        for up in (True, False):
+            match = jnp.logical_and(gets(up, 0), jnp.logical_not(neighbour(up)))
+
+            @pl.when(jnp.logical_and(match, where))
+            def _():
+                o_take(up, 0, s - step_of(up), pieces)
+
+    def project(group):
+        at = slice(groups[group][0] * KEY, groups[group][1] * KEY)
+        from_late = span_at(late_source, depth)
+        with scope(f"wait_w{group}"):
+            block = weights.at[pl.ds(0, half), at]
+            tally(block, wy_out, wy_in.at[1 + group]).wait_recv()
+
+        def one(q, carry):
+            more = jnp.dot(
+                acts[q, :, from_late], weights[from_late, at], preferred_element_type=f32
+            )
+            proj[q, :, at] = (begun[q, :, at] + more).astype(bf16)
+            return carry
+
+        with scope(f"project{group}"):
+            lax.fori_loop(0, seqs, one, 0)
+
+    def begin(q, carry):
+        total = None
+        for i in range(1, n_sp):
+            rows_now = span_at(lax.rem(late_source + i, n_sp), depth)
+            more = jnp.dot(acts[q, :, rows_now], weights[rows_now, :], preferred_element_type=f32)
+            total = more if total is None else total + more
+        begun[q] = total
+        return carry
 
     with scope("joined"):
         tally(acts.at[pl.ds(0, seqs // CORES)], ac_out, ac_in).wait_recv()
         here = weights.at[own_rows, :]
         pltpu.make_async_copy(here, here, load_sem.at[2]).wait()
-
-    def project(group):
-        with scope(f"wait_w{group}"):
-            block = weights.at[pl.ds(0, last * half), w_cols(group)]
-            tally(block, wy_out, wy_in.at[group]).wait_recv()
-        at = slice(groups[group][0] * KEY, groups[group][1] * KEY)
-
-        def one(q, carry):
-            proj[q, :, at] = jnp.dot(
-                acts[q], weights[:, at], preferred_element_type=f32
-            ).astype(bf16)
-            return carry
-
-        with scope(f"project{group}"):
-            lax.fori_loop(0, seqs, one, 0)
-
+    with scope("wait_w"):
+        tally(weights.at[pl.ds(0, (last - 1) * half), :], wy_out, wy_in.at[0]).wait_recv()
+    with scope("take_part_end"):
+        take_late(range(BITS // 2), at_end)
+    with scope("begin"):
+        lax.fori_loop(0, seqs, begin, 0)
+    for group in every_group:
+        with scope(f"swap_late{group}"):
+            swap_late(group)
+    with scope("take_rest_end"):
+        take_late(range(BITS // 2, BITS), at_end)
     project(0)
+    project(1)
     with scope("act_drain"):
         tally(acts.at[:, pl.ds(0, n_sp * span), :], ax_out, ax_in.at[0]).wait_send()
         tally(acts.at[pl.ds(0, seqs // CORES)], ac_out, ac_in).wait_send()
@@ -663,7 +720,8 @@
                     index = slot(up, d) - 1
                     tally(block(s, t), az_out.at[index], az_in.at[index, 0]).wait_send()
 
-    project(1)
+    with scope("take_part"):
+        take_late(range(EARLY), jnp.logical_not(at_end))
     project(2)
     with scope("wait_shift"):
         tally(shifts.at[:, pl.ds(0, last * positions), :], sz_out, sz_in).wait_recv()
@@ -675,95 +733,148 @@
             mixed.at[q, z_at[k], :, core_at[o]],
             heads.at[:, q, :, lanes(c * n_sp + s, VAL)],
             m_out,
-            m_in,
+            m_in.at[q // lot],
             (g, z_at[k], x * CORES + core_at[o]),
         )
 
-    def recur(q, carry):
-        value = recur_one(proj, shifts, gap_ref, gain_ref, summed, q, lanes(s))
-        mixed[q] = value.reshape(n_sp, n_x, CORES, span, VAL)
-        heads[:, q, :, lanes(c * n_sp + s, VAL)] = mixed[q, s, :, c]
+    def send_mixed(seqs_now, held):
         for k, o in targets:
-            m_move(q, k, o).start()
+            crossing = jnp.logical_and(at_end, jnp.abs(z_at[k] - s) > HOLD)
+
+            @pl.when(crossing if held else jnp.logical_not(crossing))
+            def _():
+                for q in seqs_now:
+                    m_move(q, k, o).start()
+
+    def recur(pair, carry):
+        for i in range(2):
+            q = 2 * pair + i
+            value = recur_one(proj, shifts, gap_ref, gain_ref, summed.at[i], q, lanes(s))
+            mixed[q] = value.reshape(n_sp, n_x, CORES, span, VAL)
+            heads[:, q, :, lanes(c * n_sp + s, VAL)] = mixed[q, s, :, c]
+        send_mixed(range(2 * pair, 2 * pair + 2), False)
         return carry
 
-    with scope("recur"):
-        lax.fori_loop(0, seqs, recur, 0)
-    with scope("forward"):
+    def take_second(pieces, where):
         for up in (True, False):
 
-            @pl.when(jnp.logical_and(neighbour(up), sends(up, 1)))
+            @pl.when(jnp.logical_and(gets(up, 1), where))
             def _():
-                for piece in range(PIECES):
-                    o_z(up, 1, piece).start()
-
+                o_take(up, 1, s - 2 * step_of(up), pieces)
+
+    def take_third(pieces):
+        each(last - 1, lambda up, d, origin: o_take(up, d, origin, pieces))
+
+    for pair in range(seqs // 2):
+        with scope(f"recur{pair}"):
+            recur(pair, 0)
+        if pair == 0:
+            with scope("take_second"):
+                take_second(range(EARLY), at_end)
     with scope("take_late"):
-        for up in (True, False):
-
-            @pl.when(jnp.logical_and(gets(up, 0), jnp.logical_not(neighbour(up))))
-            def _():
-                o_take(up, 0, s - step_of(up))
-
+        take_late(range(EARLY, BITS), jnp.logical_not(at_end))
     with scope("w_drain"):
         tally(own_shift.at[pl.ds(0, last)], sz_out, sz_in).wait_send()
         every = weights.at[pl.ds(0, last * half), :]
         tally(every, wz_out, wz_in.at[0, 0]).wait_send()
         tally(every, wy_out, wy_in.at[0]).wait_send()
-    for d in range(1, last):
-        with scope(f"o_swapped{d - 1}"):
-            each(d - 1, o_swapped)
-        with scope(f"o_pass{d}"):
-            each(d, o_take)
     w_own.wait()
 
-    def p_move(index, origin):
+    def p_move(index, origin, rows_now, part):
         at = lanes(origin, width)
-        peer = (g, s, across)
-        return remote(partial.at[1 - x, :, :, at], landed.at[:, :, at], p_out, p_in.at[index], peer)
-
-    def strip(index, origin):
+        return remote(
+            partial.at[1 - x, rows_now, :, at],
+            landed.at[rows_now, :, at],
+            p_out,
+            p_in.at[index, part],
+            (g, s, across),
+        )
+
+    every_seq = (slice(0, seqs),)
+    lots = tuple(slice(h * lot, (h + 1) * lot) for h in range(PIECES))
+
+    def strip(index, origin, rows_now, part):
+        at = lanes(origin, width)
+        lines = heads[:, rows_now].reshape(-1, heads.shape[-1])
+        partial[:, rows_now, :, at] = (
+            jnp.dot(lines, matrix[:, at], preferred_element_type=f32)
+            .astype(bf16)
+            .reshape(n_x, -1, span, width)
+        )
+        p_move(index, origin, rows_now, part).start()
+
+    def arrived_strip(index, origin):
         at = lanes(origin, width)
         tally(matrix.at[pl.ds(0, depth), at], oc_out, oc_in.at[index]).wait_recv()
-        lines = heads[...].reshape(n_x * seqs * span, -1)
-        partial[:, :, :, at] = (
-            jnp.dot(lines, matrix[:, at], preferred_element_type=f32)
-            .astype(bf16)
-            .reshape(n_x, seqs, span, width)
-        )
-        p_move(index, origin).start()
-
-    def o_strip(up, d, origin):
-        strip(slot(up, d), origin)
-
-    all_mixed = tally(heads.at[:, :, :, pl.ds(0, len(targets) * VAL)], m_out, m_in)
-    with scope("wait_m"):
-        all_mixed.wait_recv()
-    with scope("own_strip"):
-        strip(0, s)
-    for d in range(last - 1):
+
+    def own_strip(part):
+        strip(0, s, lots[part], part)
+
+    def near_strip(part):
+        def visit(up, d, origin):
+            if part == 0:
+                arrived_strip(slot(up, d), origin)
+            strip(slot(up, d), origin, lots[part], part)
+
+        each(0, visit)
+
+    def far_strip(up, d, origin):
+        arrived_strip(slot(up, d), origin)
+        strip(slot(up, d), origin, every_seq[0], 0)
+
+    def mixed_in(part):
+        here = heads.at[:, pl.ds(0, lot), :, pl.ds(0, len(targets) * VAL)]
+        tally(here, m_out, m_in.at[part]).wait_recv()
+
+    with scope("o_pass1"):
+        take_second(range(EARLY, BITS), at_end)
+        send_mixed(range(seqs), True)
+        take_second(range(BITS), jnp.logical_not(at_end))
+    with scope("o_pass2a"):
+        take_third(range(BITS // 2))
+    with scope("o_swapped0"):
+        each(0, o_swapped)
+    with scope("wait_m0"):
+        mixed_in(0)
+    with scope("own_strip0"):
+        arrived_strip(0, s)
+        own_strip(0)
+    with scope("near_strip0"):
+        near_strip(0)
+    with scope("o_pass2b"):
+        take_third(range(BITS // 2, BITS))
+    with scope("wait_m1"):
+        for part in range(1, PIECES):
+            mixed_in(part)
+    with scope("strips1"):
+        for part in range(1, PIECES):
+            own_strip(part)
+            near_strip(part)
+    for d in range(1, last):
+        with scope(f"o_swapped{d}"):
+            each(d, o_swapped)
         with scope(f"strip{d}"):
-            each(d, o_strip)
-    with scope(f"o_swapped{last - 1}"):
-        each(last - 1, o_swapped)
-    with scope(f"strip{last - 1}"):
-        each(last - 1, o_strip)
-
-    def finish(index, origin):
-        p_move(index, origin).wait_recv()
-        at = lanes(origin, width)
-        total = partial[x, :, :, at].astype(f32) + landed[:, :, at].astype(f32)
-        out_ref[:, :, at] = total.astype(bf16)
+            each(d, far_strip)
+
+    def finish(index, origin, parts):
+        for part, rows_now in enumerate(parts):
+            p_move(index, origin, rows_now, part).wait_recv()
+            at = lanes(origin, width)
+            total = partial[x, rows_now, :, at].astype(f32) + landed[rows_now, :, at].astype(f32)
+            out_ref[rows_now, :, at] = total.astype(bf16)
 
     with scope("finish"):
-        finish(0, s)
+        finish(0, s, lots)
         for d in range(last):
-            each(d, lambda up, d, origin: finish(slot(up, d), origin))
+            parts = every_seq if d else lots
+            each(d, lambda up, d, origin: finish(slot(up, d), origin, parts))
     with scope("drain"):
-        all_mixed.wait_send()
+        here = heads.at[:, :, :, pl.ds(0, len(targets) * VAL)]
+        tally(here, m_out, m_in.at[0]).wait_send()
         strips = matrix.at[pl.ds(0, half), pl.ds(0, last * width)]
         tally(strips, oy_out, oy_in.at[0, 0]).wait_send()
         tally(matrix.at[pl.ds(0, depth), :], oc_out, oc_in.at[0]).wait_send()
-        tally(landed, p_out, p_in.at[0]).wait_send()
+        tally(landed, p_out, p_in.at[0, 0]).wait_send()
         for d in range(last):
             for up in (True, False):
 
@@ -799,8 +910,9 @@
             pltpu.VMEM((seqs, length, KEY), bf16),
             pltpu.VMEM((seqs, length, model), bf16),
             pltpu.VMEM((model, count * KEY), bf16),
+            pltpu.VMEM((seqs, length, count * KEY), jnp.float32),
             pltpu.VMEM((seqs, length, count * KEY), bf16),
-            pltpu.VMEM((length, VAL), jnp.float32),
+            pltpu.VMEM((2, length, VAL), jnp.float32),
             pltpu.VMEM((seqs, n_sp, n_x, CORES, span, VAL), bf16),
             pltpu.VMEM((n_x, seqs, span, CORES * depth), bf16),
             pltpu.VMEM((CORES * depth, n_sp * width), bf16),
@@ -814,21 +926,21 @@
             dma,
             dma,
             dma,
-            dma((n_sp - 1, 3)),
+            dma((n_sp - 1, count)),
             dma,
-            dma((3,)),
+            dma((4,)),
             dma,
             dma,
             dma((slots - 1,)),
-            dma((slots - 1, PIECES)),
+            dma((slots - 1, BITS)),
             dma,
-            dma((slots - 1, PIECES)),
+            dma((slots - 1, BITS)),
             dma,
             dma((slots,)),
             dma,
+            dma((PIECES,)),
             dma,
-            dma,
-            dma((slots,)),
+            dma((slots, PIECES)),
         ],
         compiler_params=pltpu.CompilerParams(
             collective_id=0, has_side_effects=True, vmem_limit_bytes=56 * 1024 * 1024
@@ -870,7 +982,7 @@
         heads_here = w_query.shape[1] // KEY // n_tp
         span = tokens.shape[0] // (n_sp * n_tp)
         sizes = (mesh.shape["grp"], n_sp, n_tp)
-        fits = heads_here == n_sp and n_sp > 2 and n_tp == 2 * CORES and span % 16 == 0
+        fits = heads_here == n_sp and n_sp == CORES * 2 and n_tp == 2 * CORES and span % 16 == 0
         fits = fits and sizes[0] == 2 and tokens.shape[1] // sizes[0] % PIECES == 0
         fits = fits and tokens.shape[0] % BLOCK == 0 and tokens.shape[0] <= 512
         body = functools.partial(head_shards, sizes) if fits else shards

time: 87.1 us -> 84.6 us (0.971)
  Pallas kernels: 85 us -> 82.5 us
    pallas_call x1, Pallas kernels: 85 us -> 82.5 us  [layer(): pl.pallas_call(functools.partial(layer_kernel, sizes), out_shape=jax.Shap...]
where the time goes in v3:
time: 84.6 us; the launch traced here: 84.4 us
  Pallas kernels  82.5 us (98%)
  local copies, waits for them, and re-layouts  1.86 us (2%)
    pallas_call x1, Pallas kernels, layer(): pl.pallas_call(functools.partial(layer_kernel, sizes), out_shape=jax.Shap...  82.5 us
    transpose x1, local copies, waits for them, and re-layouts, head_shards(): return layer(sizes, tokens, norm_gain.reshape(1, 1, -1), decay_shift, (w_...  1.86 us

profile of v3, /device:TPU:0, one launch (start us, length us, event | category | flops | bytes accessed | tf_op | source)
XLA Modules:
  0.0 84.4 jit_solution(4393775335025696099)
XLA Ops:
  0.0 82.5 %shard_map.109 = bf16[4,16,2048]{2,1,0:T(8,128)(2,1)} custom-call(bf16[16,4,2048]{2,1,0:T(4,128)(2,1)} %token_ref.1, f32[1,1,2048]{2,1,0:T(1,128)} %bitcast.4, f32[64,4,512]{2,1,0:T(4,128)} %shift_ref.1, bf16[512,512]{1,0:T(8,128)(2,1)} %wq_ref.1, bf16[512,512]{1,0:T(8,128)(2,1)} %wv_ref.1, bf16[512,512]{1,0:T(8,128)(2,1)} %wf_ref.1, ...), custom_call_target="tpu_custom_call" | custom-call | tf_op jit(solution)/shard_map/pallas_call | solution.py:900
  82.5 1.9 %copy.12 = bf16[16,4,2048]{2,1,0:T(4,128)(2,1)} copy(bf16[16,4,2048]{2,0,1:T(8,128)(2,1)} %bitcast.3) | data formatting | bytes 524288 | tf_op jit(solution)/shard_map/transpose | solution.py:974

commit v4 on v3

--- a/solution.py
+++ b/solution.py
@@ -206,8 +206,8 @@
 CORES = 2
 PIECES = 2
 BITS = 4
-EARLY = 2
-HOLD = 5
+EARLY = 3
+FREE = 1
 scope = jax.named_scope
 
 
@@ -737,14 +737,24 @@
             (g, z_at[k], x * CORES + core_at[o]),
         )
 
-    def send_mixed(seqs_now, held):
+    def send_mixed(pair, stage):
         for k, o in targets:
-            crossing = jnp.logical_and(at_end, jnp.abs(z_at[k] - s) > HOLD)
-
-            @pl.when(crossing if held else jnp.logical_not(crossing))
+            to_end = jnp.logical_or(z_at[k] == 0, z_at[k] == last)
+            to_end = jnp.logical_and(to_end, k > 0)
+            far = jnp.logical_and(to_end, jnp.abs(z_at[k] - s) > 1)
+            if pair < FREE:
+                match = stage == 0
+            elif stage == 0:
+                match = jnp.logical_not(to_end)
+            elif stage == 1:
+                match = jnp.logical_and(to_end, jnp.logical_not(far))
+            else:
+                match = far
+
+            @pl.when(match)
             def _():
-                for q in seqs_now:
-                    m_move(q, k, o).start()
+                for i in range(2):
+                    m_move(2 * pair + i, k, o).start()
 
     def recur(pair, carry):
         for i in range(2):
@@ -752,7 +762,7 @@
             value = recur_one(proj, shifts, gap_ref, gain_ref, summed.at[i], q, lanes(s))
             mixed[q] = value.reshape(n_sp, n_x, CORES, span, VAL)
             heads[:, q, :, lanes(c * n_sp + s, VAL)] = mixed[q, s, :, c]
-        send_mixed(range(2 * pair, 2 * pair + 2), False)
+        send_mixed(pair, 0)
         return carry
 
     def take_second(pieces, where):
@@ -790,7 +800,6 @@
             (g, s, across),
         )
 
-    every_seq = (slice(0, seqs),)
     lots = tuple(slice(h * lot, (h + 1) * lot) for h in range(PIECES))
 
     def strip(index, origin, rows_now, part):
@@ -810,17 +819,13 @@
     def own_strip(part):
         strip(0, s, lots[part], part)
 
-    def near_strip(part):
+    def other_strip(d, part):
         def visit(up, d, origin):
             if part == 0:
                 arrived_strip(slot(up, d), origin)
             strip(slot(up, d), origin, lots[part], part)
 
-        each(0, visit)
-
-    def far_strip(up, d, origin):
-        arrived_strip(slot(up, d), origin)
-        strip(slot(up, d), origin, every_seq[0], 0)
+        each(d, visit)
 
     def mixed_in(part):
         here = heads.at[:, pl.ds(0, lot), :, pl.ds(0, len(targets) * VAL)]
@@ -828,10 +833,15 @@
 
     with scope("o_pass1"):
         take_second(range(EARLY, BITS), at_end)
-        send_mixed(range(seqs), True)
         take_second(range(BITS), jnp.logical_not(at_end))
+    for pair in range(FREE, seqs // 2):
+        send_mixed(pair, 1)
     with scope("o_pass2a"):
         take_third(range(BITS // 2))
+    for pair in range(FREE, seqs // 2):
+        send_mixed(pair, 2)
+    with scope("o_pass2b"):
+        take_third(range(BITS // 2, BITS))
     with scope("o_swapped0"):
         each(0, o_swapped)
     with scope("wait_m0"):
@@ -840,21 +850,19 @@
         arrived_strip(0, s)
         own_strip(0)
     with scope("near_strip0"):
-        near_strip(0)
-    with scope("o_pass2b"):
-        take_third(range(BITS // 2, BITS))
-    with scope("wait_m1"):
-        for part in range(1, PIECES):
-            mixed_in(part)
-    with scope("strips1"):
-        for part in range(1, PIECES):
-            own_strip(part)
-            near_strip(part)
+        other_strip(0, 0)
     for d in range(1, last):
         with scope(f"o_swapped{d}"):
             each(d, o_swapped)
         with scope(f"strip{d}"):
-            each(d, far_strip)
+            other_strip(d, 0)
+    for part in range(1, PIECES):
+        with scope(f"wait_m{part}"):
+            mixed_in(part)
+        with scope(f"strips{part}"):
+            own_strip(part)
+            for d in range(last):
+                other_strip(d, part)
 
     def finish(index, origin, parts):
         for part, rows_now in enumerate(parts):
@@ -866,8 +874,7 @@
     with scope("finish"):
         finish(0, s, lots)
         for d in range(last):
-            parts = every_seq if d else lots
-            each(d, lambda up, d, origin: finish(slot(up, d), origin, parts))
+            each(d, lambda up, d, origin: finish(slot(up, d), origin, lots))
     with scope("drain"):
         here = heads.at[:, :, :, pl.ds(0, len(targets) * VAL)]
         tally(here, m_out, m_in.at[0]).wait_send()
@@ -943,7 +950,7 @@
             dma((slots, PIECES)),
         ],
         compiler_params=pltpu.CompilerParams(
-            collective_id=0, has_side_effects=True, vmem_limit_bytes=56 * 1024 * 1024
+            collective_id=0, has_side_effects=True, vmem_limit_bytes=107 * 512 * 1024
         ),
     )(tokens, norm_gain, shift, *sources, gap, gain, w_out)
 

time: 84.6 us -> 83.3 us (0.985)
  Pallas kernels: 82.5 us -> 80.1 us
  local copies, waits for them, and re-layouts: 1.86 us -> 2.95 us
    pallas_call x1, Pallas kernels: 82.5 us -> 80.1 us  [layer(): pl.pallas_call(functools.partial(layer_kernel, sizes), out_shape=jax.Shap...]
    unnamed x0 -> x6, local copies, waits for them, and re-layouts: none -> 2.04 us
    transpose x1, local copies, waits for them, and re-layouts: 1.86 us -> 0.91 us  [head_shards(): return layer(sizes, tokens, norm_gain.reshape(1, 1, -1), decay_shift, (w_...]
where the time goes in v4:
time: 83.3 us; the launch traced here: 83.1 us
  Pallas kernels  80.1 us (96%)
  local copies, waits for them, and re-layouts  2.95 us (4%)
    pallas_call x1, Pallas kernels, layer(): pl.pallas_call(functools.partial(layer_kernel, sizes), out_shape=jax.Shap...  80.1 us
    unnamed x6, local copies, waits for them, and re-layouts  2.04 us

profile of v4, /device:TPU:0, one launch (start us, length us, event | category | flops | bytes accessed | tf_op | source)
XLA Modules:
  0.0 83.1 jit_solution(10478433171393812902)
XLA Ops:
  0.0 0.0 copy-start.2
  0.0 0.7 copy-done.2
  0.7 0.0 copy-start
  0.7 0.7 copy-done
  1.4 0.0 copy-start.1
  1.4 0.7 copy-done.1
  2.0 80.1 %shard_map.109 = bf16[4,16,2048]{2,1,0:T(8,128)(2,1)S(1)} custom-call(bf16[16,4,2048]{2,1,0:T(4,128)(2,1)} %token_ref.1, f32[1,1,2048]{2,1,0:T(1,128)S(1)} %bitcast.4, f32[64,4,512]{2,1,0:T(4,128)} %shift_ref.1, bf16[512,512]{1,0:T(8,128)(2,1)} %wq_ref.1, bf16[512,512]{1,0:T(8,128)(2,1)} %wv_ref.1, bf16[512,512]{1,0:T(8,128)(2,1)} %wf_ref.1, ...), custom_call_target="tpu_custom_call" | custom-call | tf_op jit(solution)/shard_map/pallas_call | solution.py:907
  82.2 0.9 %copy.12 = bf16[16,4,2048]{2,1,0:T(4,128)(2,1)} copy(bf16[16,4,2048]{2,0,1:T(8,128)(2,1)S(1)} %bitcast.3) | data formatting | bytes 524288 | tf_op jit(solution)/shard_map/transpose | solution.py:981
Async XLA Ops:
  0.0 0.7 copy-start.2
  0.7 0.7 copy-start
  1.4 0.7 copy-start.1

commit v5 on v4

--- a/solution.py
+++ b/solution.py
@@ -207,6 +207,8 @@
 PIECES = 2
 BITS = 4
 EARLY = 3
+VL = 56
+TRIG = 2
 FREE = 1
 scope = jax.named_scope
 
@@ -290,17 +292,20 @@
 def layer_kernel(
     sizes,
     token_ref,
-    norm_ref,
+    norm_hbm,
     shift_ref,
     wq_ref,
     wv_ref,
     wf_ref,
     wb_ref,
     wg_ref,
+    gap_hbm,
+    gain_hbm,
+    w_ref,
+    out_ref,
+    norm_ref,
     gap_ref,
     gain_ref,
-    w_ref,
-    out_ref,
     rows_in,
     wide,
     raw_shift,
@@ -414,6 +419,14 @@
     load_rows = pltpu.make_async_copy(token_ref, rows_in, load_sem.at[0])
     load_shift = pltpu.make_async_copy(shift_ref, raw_shift, load_sem.at[1])
     load_rows.start()
+    small = [
+        pltpu.make_async_copy(src, dst, load_sem.at[4 + i])
+        for i, (src, dst) in enumerate(
+            ((norm_hbm, norm_ref), (gap_hbm, gap_ref), (gain_hbm, gain_ref))
+        )
+    ]
+    for copy in small:
+        copy.start()
     load_shift.start()
     peers = [(g, z_at[k], x * CORES + core_at[o]) for k in range(n_sp) for o in range(CORES)]
     peers = peers[1:] + [(g, s, across), (1 - g, s, t)]
@@ -432,6 +445,8 @@
     here_rows = span_at(s * n_tp + t, span)
     with scope("wait_rows"):
         load_rows.wait()
+        for copy in small:
+            copy.wait()
     rows = rows_in[...].astype(f32)
     scale = lax.rsqrt(jnp.mean(rows * rows, axis=-1, keepdims=True) + norm_eps)
     wide[...] = rows * scale * norm_ref[...]
@@ -571,29 +586,28 @@
         def _():
             issue(up)
 
-    def swap(d, groups_now, match=True, late=False):
+    def swap(d, pieces, match=True, late=None):
         for up in (True, False):
 
             @pl.when(jnp.logical_and(gets(up, d), match))
             def _():
                 k = d + 1 if up else last - d
-                for group in groups_now:
-                    for p in range(*groups[group]):
-                        tally(w_block(k, p), wz_out, wz_in.at[k - 1, p]).wait_recv()
-                        w_y(k, p, 1 + group if late else 0).start()
+                for p in pieces:
+                    tally(w_block(k, p), wz_out, wz_in.at[k - 1, p]).wait_recv()
+                    w_y(k, p, 0 if late is None else 1 + late).start()
 
     at_end = jnp.logical_or(s == 0, s == last)
     late_source = jnp.where(at_end, last - s, lax.rem(s + 2, n_sp))
 
     def swap_late(group):
-        swap(last - 1, (group,), at_end, True)
-        swap(last - 2, (group,), jnp.logical_not(at_end), True)
+        swap(last - 1, range(*groups[group]), at_end, group)
+        swap(last - 2, range(*groups[group]), jnp.logical_not(at_end), group)
 
     for d in range(last):
         if d == last - 1:
             with scope("swap_end"):
                 for hop in range(last - 2, 0, -1):
-                    swap(hop, every_group, at_end)
+                    swap(hop, range(count), at_end)
         for piece in range(PIECES):
 
             def arrived(up, d, origin):
@@ -649,10 +663,10 @@
                 o_take(up, 0, s - step_of(up))
 
     with scope("swap_near0"):
-        swap(0, every_group[:1])
+        swap(0, range(TRIG))
     issue_far()
     with scope("swap_near1"):
-        swap(0, every_group[1:])
+        swap(0, range(TRIG, count))
     with scope("relay"):
         relay(0, s)
         for d in range(last):
@@ -840,10 +854,17 @@
         take_third(range(BITS // 2))
     for pair in range(FREE, seqs // 2):
         send_mixed(pair, 2)
-    with scope("o_pass2b"):
-        take_third(range(BITS // 2, BITS))
+    def second_swapped(where):
+        for up in (True, False):
+
+            @pl.when(jnp.logical_and(gets(up, 1), where))
+            def _():
+                o_swapped(up, 1, s - 2 * step_of(up))
+
     with scope("o_swapped0"):
         each(0, o_swapped)
+    with scope("o_swapped1e"):
+        second_swapped(at_end)
     with scope("wait_m0"):
         mixed_in(0)
     with scope("own_strip0"):
@@ -851,17 +872,22 @@
         own_strip(0)
     with scope("near_strip0"):
         other_strip(0, 0)
-    for d in range(1, last):
-        with scope(f"o_swapped{d}"):
-            each(d, o_swapped)
-        with scope(f"strip{d}"):
-            other_strip(d, 0)
+    with scope("o_pass2b"):
+        take_third(range(BITS // 2, BITS))
     for part in range(1, PIECES):
         with scope(f"wait_m{part}"):
             mixed_in(part)
         with scope(f"strips{part}"):
             own_strip(part)
-            for d in range(last):
+            other_strip(0, part)
+    with scope("o_swapped1m"):
+        second_swapped(jnp.logical_not(at_end))
+    for d in range(1, last):
+        if d > 1:
+            with scope(f"o_swapped{d}"):
+                each(d, o_swapped)
+        with scope(f"strip{d}"):
+            for part in range(PIECES):
                 other_strip(d, part)
 
     def finish(index, origin, parts):
@@ -907,9 +933,12 @@
     return pl.pallas_call(
         functools.partial(layer_kernel, sizes),
         out_shape=jax.ShapeDtypeStruct((seqs, span, n_sp * width), bf16),
-        in_specs=[hbm, vmem] + [hbm] * (1 + count) + [vmem, vmem, hbm],
+        in_specs=[hbm] * (6 + count),
         out_specs=vmem,
         scratch_shapes=[
+            pltpu.VMEM(norm_gain.shape, norm_gain.dtype),
+            pltpu.VMEM(gap.shape, gap.dtype),
+            pltpu.VMEM(gain.shape, gain.dtype),
             pltpu.VMEM(tokens.shape, bf16),
             pltpu.VMEM(tokens.shape, jnp.float32),
             pltpu.VMEM(shift.shape, shift.dtype),
@@ -925,7 +954,7 @@
             pltpu.VMEM((CORES * depth, n_sp * width), bf16),
             pltpu.VMEM((n_x, seqs, span, n_sp * width), bf16),
             pltpu.VMEM((seqs, span, n_sp * width), bf16),
-            dma((4,)),
+            dma((7,)),
             dma((slots - 1,)),
             dma((slots - 1, PIECES)),
             dma,
@@ -950,7 +979,7 @@
             dma((slots, PIECES)),
         ],
         compiler_params=pltpu.CompilerParams(
-            collective_id=0, has_side_effects=True, vmem_limit_bytes=107 * 512 * 1024
+            collective_id=0, has_side_effects=True, vmem_limit_bytes=int(VL * 1024 * 1024)
         ),
     )(tokens, norm_gain, shift, *sources, gap, gain, w_out)
 

time: 83.3 us -> 82.9 us (level)
  local copies, waits for them, and re-layouts: 2.95 us -> 1.86 us
    unnamed x6 -> x0, local copies, waits for them, and re-layouts: 2.04 us -> none
    transpose x1, local copies, waits for them, and re-layouts: 0.91 us -> 1.86 us  [head_shards(): return layer(sizes, tokens, norm_gain.reshape(1, 1, -1), decay_shift, (w_...]
where the time goes in v5:
time: 82.9 us; the launch traced here: 82.8 us
  Pallas kernels  80.9 us (98%)
  local copies, waits for them, and re-layouts  1.86 us (2%)
    pallas_call x1, Pallas kernels, layer(): pl.pallas_call(functools.partial(layer_kernel, sizes), out_shape=jax.Shap...  80.9 us
    transpose x1, local copies, waits for them, and re-layouts, head_shards(): return layer(sizes, tokens, norm_gain.reshape(1, 1, -1), decay_shift, (w_...  1.86 us

profile of v5, /device:TPU:0, one launch (start us, length us, event | category | flops | bytes accessed | tf_op | source)
XLA Modules:
  0.0 82.8 jit_solution(13413420516817850035)
XLA Ops:
  0.0 80.9 %shard_map.109 = bf16[4,16,2048]{2,1,0:T(8,128)(2,1)} custom-call(bf16[16,4,2048]{2,1,0:T(4,128)(2,1)} %token_ref.1, f32[1,1,2048]{2,1,0:T(1,128)} %bitcast.4, f32[64,4,512]{2,1,0:T(4,128)} %shift_ref.1, bf16[512,512]{1,0:T(8,128)(2,1)} %wq_ref.1, bf16[512,512]{1,0:T(8,128)(2,1)} %wv_ref.1, bf16[512,512]{1,0:T(8,128)(2,1)} %wf_ref.1, ...), custom_call_target="tpu_custom_call" | custom-call | tf_op jit(solution)/shard_map/pallas_call | solution.py:933
  80.9 1.9 %copy.12 = bf16[16,4,2048]{2,1,0:T(4,128)(2,1)} copy(bf16[16,4,2048]{2,0,1:T(8,128)(2,1)} %bitcast.3) | data formatting | bytes 524288 | tf_op jit(solution)/shard_map/transpose | solution.py:1010

commit v6 on v5

--- a/solution.py
+++ b/solution.py
@@ -505,7 +505,7 @@
 
     def o_y(index, origin, piece):
         here = o_block(origin, g, c, piece)
-        return remote(here, here, oy_out, oy_in.at[index - 1, piece], (1 - g, s, t))
+        return remote(here, here, oy_out, oy_in.at[index - 1, piece // 2], (1 - g, s, t))
 
     def o_c(far, index, origin, piece):
         here = o_block(origin, 1 - g if far else g, c, piece)
@@ -651,9 +651,12 @@
             o_c(0, slot(up, d), origin, piece).start()
 
     def o_swapped(up, d, origin):
-        for piece in range(BITS):
-            o_y(slot(up, d), origin, piece).wait_recv()
-            o_c(1, slot(up, d), origin, piece).start()
+        for first in range(0, BITS, 2):
+            at = pl.multiple_of(c * depth + (1 - g) * half + first * bit, bit)
+            here = matrix.at[pl.ds(at, 2 * bit), lanes(origin, width)]
+            index = slot(up, d)
+            tally(here, oy_out, oy_in.at[index - 1, first // 2]).wait_recv()
+            remote(here, here, oc_out, oc_in.at[index], (g, s, twin)).start()
 
     with scope("take_early"):
         for up in (True, False):
@@ -970,7 +973,7 @@
             dma((slots - 1,)),
             dma((slots - 1, BITS)),
             dma,
-            dma((slots - 1, BITS)),
+            dma((slots - 1, BITS // 2)),
             dma,
             dma((slots,)),
             dma,

time: 82.9 us -> 82.8 us (level)
  no operation moved by 1% of the time
where the time goes in v6:
time: 82.8 us; the launch traced here: 82.6 us
  Pallas kernels  80.8 us (98%)
  local copies, waits for them, and re-layouts  1.86 us (2%)
    pallas_call x1, Pallas kernels, layer(): pl.pallas_call(functools.partial(layer_kernel, sizes), out_shape=jax.Shap...  80.8 us
    transpose x1, local copies, waits for them, and re-layouts, head_shards(): return layer(sizes, tokens, norm_gain.reshape(1, 1, -1), decay_shift, (w_...  1.86 us

profile of v6, /device:TPU:0, one launch (start us, length us, event | category | flops | bytes accessed | tf_op | source)
XLA Modules:
  0.0 82.6 jit_solution(5790181297886494574)
XLA Ops:
  0.0 80.8 %shard_map.109 = bf16[4,16,2048]{2,1,0:T(8,128)(2,1)} custom-call(bf16[16,4,2048]{2,1,0:T(4,128)(2,1)} %token_ref.1, f32[1,1,2048]{2,1,0:T(1,128)} %bitcast.4, f32[64,4,512]{2,1,0:T(4,128)} %shift_ref.1, bf16[512,512]{1,0:T(8,128)(2,1)} %wq_ref.1, bf16[512,512]{1,0:T(8,128)(2,1)} %wv_ref.1, bf16[512,512]{1,0:T(8,128)(2,1)} %wf_ref.1, ...), custom_call_target="tpu_custom_call" | custom-call | tf_op jit(solution)/shard_map/pallas_call | solution.py:936
  80.8 1.9 %copy.12 = bf16[16,4,2048]{2,1,0:T(4,128)(2,1)} copy(bf16[16,4,2048]{2,0,1:T(8,128)(2,1)} %bitcast.3) | data formatting | bytes 524288 | tf_op jit(solution)/shard_map/transpose | solution.py:1013
